TPU v7x, 256 devices: a 4x2x16 block of a 4x16x16 slice. The times are simulated.
256 devices in a mesh: grp: 2 (over y), tp: 16 (over z), dp: 8 (over x, core).
Axes of the slice: x: 4, y: 2, z: 16, core: 2. Of those that a mesh axis runs over, the one named last changes fastest.
The devices are a block of a 4x16x16 slice.
Arguments:
- tokens: bfloat16 [256, 4096], P('grp', 'dp'), parts along dimension 0, may hold values from -50 to 50
- lengths: int32 [256], P(('grp', 'dp')), parts along dimension 0, may hold values from 1 to 24, as said below
- norm_gain: float32 [2, 4096], P(None, 'dp'), may hold values from 0.1 to 1.9
- w_z: bfloat16 [2, 4096, 4096], P(None, 'dp', 'tp'), may hold values from -0.09375 to 0.09375
- w_x: bfloat16 [2, 4096, 4096], P(None, 'dp', 'tp'), may hold values from -0.09375 to 0.09375
- w_b: bfloat16 [2, 4096, 2048], P(None, 'dp', 'tp'), may hold values from -0.09375 to 0.09375
- w_c: bfloat16 [2, 4096, 2048], P(None, 'dp', 'tp'), may hold values from -0.09375 to 0.09375
- w_dt: bfloat16 [2, 4096, 64], P(None, 'dp'), may hold values from -0.09375 to 0.09375
- conv_weight: bfloat16 [2, 4, 8192], P(None, None, 'tp'), may hold values from -3 to 3
- dt_bias: float32 [2, 64], P(None, 'tp'), may hold values from -6 to -1.5
- a_log: float32 [2, 64], P(None, 'tp'), may hold values from 0 to 2.77
- d_skip: float32 [2, 64], P(None, 'tp'), may hold values from 0.1 to 1.9
- out_gain: float32 [2, 4096], P(None, 'tp'), may hold values from 0.1 to 1.9
- w_out: bfloat16 [2, 4096, 4096], P(None, 'tp', 'dp'), may hold values from -0.09375 to 0.09375
- conv_state: bfloat16 [2, 256, 3, 8192], P(None, ('grp', 'dp'), None, 'tp'), parts along dimension 1, may hold values from -6 to 6
- ssm_state: float32 [2, 256, 64, 64, 128], P(None, ('grp', 'dp'), 'tp'), parts along dimension 1, may hold values from -2 to 2
Outputs:
- mixed_out: bfloat16 [256, 4096], P('grp', 'dp'), parts along dimension 0
- conv_new: bfloat16 [2, 256, 3, 8192], P(None, ('grp', 'dp'), None, 'tp'), parts along dimension 1
- ssm_new: float32 [2, 256, 64, 64, 128], P(None, ('grp', 'dp'), 'tp'), parts along dimension 1
There are 2 independent parts, one for each index of `grp`. A program takes and returns all parts, laid end to end along the dimension named above; an argument that names none is the same for every part. Nothing has to cross between parts.
Inputs may be any that keep to these rules, and one draw needn't show every extreme that they name: `lengths`: each part has at least one sequence of length 24.
All inputs are finite; a program needn't handle non-finite values.
Results may differ from a plain program's by a relative error of at most 0.012.
Values may be sent and summed in bfloat16 or wider, within the bound.
No kernel may reach another device: no remote copies, remote signals or barrier semaphores. Data moves between devices by JAX's collectives and lax.ppermute only.
A program may use at most 64 MiB of HBM per device.

v0:
```python
import functools

import jax
import jax.numpy as jnp
from jax import lax
from jax.experimental import pallas as pl
from jax.experimental.pallas import tpu as pltpu
from jax.sharding import PartitionSpec as P


D = 4096
HEADS = 64
GROUPS = 16
CONV_W = 4
EPSILON = 1e-06
LANES = 128
PIECE = 16
PIECES = 4
BF16 = jnp.bfloat16
F32 = jnp.float32
MIB = 1 << 20

VMEM_SPEC = pl.BlockSpec(memory_space=pltpu.VMEM)


def params(mib):
    return pltpu.CompilerParams(vmem_limit_bytes=int(mib * MIB))


def iota(shape, dim):
    return lax.broadcasted_iota(jnp.int32, shape, dim)


def dot(a, b, dims):
    return lax.dot_general(a, b, (dims, ((), ())), preferred_element_type=F32)


def as_column(ref):
    count = ref.shape[1]
    same = iota((count, count), 0) == iota((count, count), 1)
    row = jnp.broadcast_to(ref[...].astype(F32), (count, count))
    return jnp.sum(jnp.where(same, row, 0.0), axis=1, keepdims=True)


def split(value):
    high = value.astype(BF16)
    return high, (value - high.astype(F32)).astype(BF16)


def gate_kernel(out_ref):
    out_ref[...] = jnp.zeros_like(out_ref)


def long_cost():
    return pl.CostEstimate(flops=20_000_000_000, bytes_accessed=1_000_000, transcendentals=0)


def gate():
    return pl.pallas_call(
        gate_kernel,
        out_shape=jax.ShapeDtypeStruct((8, LANES), F32),
        out_specs=VMEM_SPEC,
        compiler_params=params(1),
        cost_estimate=long_cost(),
        name="gate",
    )()


def swapped(value, mask):
    pairs = [(i, i ^ mask) for i in range(lax.axis_size("dp"))]
    return lax.ppermute(value, "dp", pairs)


def chosen_heads(heads, local_heads):
    row, column = iota((LANES, heads), 0), iota((LANES, heads), 1)
    local = row % PIECE
    first = lax.axis_index("tp") * local_heads
    return ((column == first + local) & (local < local_heads) & (row < 2 * PIECE)).astype(BF16)


def with_squares(extras, squares):
    return jnp.where(iota(extras.shape, 1) % PIECE == PIECE // 2, squares, extras)


def in_pieces(extras):
    high, low = split(extras)
    return jnp.where(iota(extras.shape, 1) < PIECE, high.astype(F32), low.astype(F32)).astype(BF16)


def block_at(k):
    at = lax.axis_index("dp")
    return lax.bitwise_xor(at // 2, jnp.int32(k)) * 2 + at % 2


def first_kernel(local_heads, block, x_ref, gain_ref, wx_ref, wb_ref, wc_ref, wz_ref, wdt_ref, _, own_ref, other_ref, *packs):
    rows, features = x_ref.shape
    blocks = [block_at(k) for k in range(rows // block // 2)]
    blocks += [lax.bitwise_xor(b, jnp.int32(1)) for b in blocks]
    tokens = [x_ref[pl.ds(pl.multiple_of(b * block, block), block), :] for b in blocks]
    wide = jnp.concatenate(tokens, axis=0).astype(F32)
    normed = (wide * gain_ref[0:1, :]).astype(BF16)
    half = rows // 2
    at = 0
    for ref in (wx_ref, wb_ref, wc_ref, wz_ref):
        width = ref.shape[-1]
        part = dot(normed, ref[0], ((1,), (0,)))
        own_ref[:, at : at + width] = part[:half]
        other_ref[:, at : at + width] = part[half:].astype(BF16)
        at += width
    chosen = chosen_heads(wdt_ref.shape[1], local_heads)
    steps = dot(wdt_ref[0], chosen, ((0,), (1,))).astype(BF16)
    squares = jnp.sum(wide * wide, axis=-1, keepdims=True)
    extras = with_squares(dot(normed, steps, ((1,), (0,))), squares)
    own_ref[:, at:] = extras[:half]
    other_ref[:, at:] = in_pieces(extras[half:])
    for layer, pack in enumerate(packs, 1):
        first = 0
        for ref in (wx_ref, wb_ref, wc_ref, wz_ref):
            pack[:features, first : first + ref.shape[-1]] = ref[layer]
            first += ref.shape[-1]
        pack[:features, at:] = dot(wdt_ref[layer], chosen, ((0,), (1,))).astype(BF16)
        row = iota((PIECE, features), 0)
        left = jnp.broadcast_to(gain_ref[layer : layer + 1, :], row.shape)
        gains = jnp.zeros_like(left)
        for k in range(3):
            piece = left.astype(BF16).astype(F32)
            gains = jnp.where(row == k, piece, gains)
            left = left - piece
        pack[features : features + PIECE, :features] = gains.astype(BF16)
        pack[features + PIECE :, :features] = x_ref[...]


def combine_kernel(own_ref, arrived_ref, *out_refs):
    total = own_ref[...] + arrived_ref[...].astype(F32)
    at = total.shape[1] - LANES
    pieces = arrived_ref[:, at:].astype(F32)
    whole = pieces + pltpu.roll(pieces, LANES - PIECE, 1)
    whole = jnp.where(iota(whole.shape, 1) < PIECE, whole, pltpu.roll(whole, PIECE, 1))
    tail = in_pieces(own_ref[:, at:] + whole)
    block = total.shape[0] // len(out_refs)
    for k, ref in enumerate(out_refs):
        ref[:, :at] = total[k * block : (k + 1) * block, :at].astype(BF16)
        ref[:, at:] = tail[k * block : (k + 1) * block]


def project_first(local_heads, block, blocks, stream, norm_gain, w_x, w_b, w_c, w_z, w_dt):
    rows, features = stream.shape
    width = sum(w.shape[2] for w in (w_x, w_b, w_c, w_z)) + LANES
    own = jax.ShapeDtypeStruct((rows // 2, width), F32)
    other = jax.ShapeDtypeStruct((rows // 2, width), BF16)
    packs = [jax.ShapeDtypeStruct((features + PIECE + rows, width), BF16)] * (w_z.shape[0] - 1)
    inputs = [stream, norm_gain, w_x, w_b, w_c, w_z, w_dt, gate()]
    own, other, *packed = pl.pallas_call(
        functools.partial(first_kernel, local_heads, block),
        out_shape=(own, other, *packs),
        in_specs=[VMEM_SPEC] * len(inputs),
        out_specs=[VMEM_SPEC] * (2 + len(packs)),
        compiler_params=params(8),
        name="project_0",
    )(*inputs)
    arrived = swapped(other, 1)
    parts = pl.pallas_call(
        combine_kernel,
        out_shape=[jax.ShapeDtypeStruct((block, width), BF16)] * blocks,
        in_specs=[VMEM_SPEC] * 2,
        out_specs=[VMEM_SPEC] * blocks,
        compiler_params=params(4),
        cost_estimate=long_cost(),
        name="combine",
    )(own, arrived)
    return parts, packed


def later_kernel(stream_ref, own_ref, other_ref, *out_refs):
    rows, features = stream_ref.shape[0] // 2, stream_ref.shape[1]
    total, squares = 0.0, 0.0
    for k, ref in enumerate((own_ref, other_ref)):
        wide = stream_ref[k * rows : (k + 1) * rows, :].astype(F32)
        pieces = ref[features : features + PIECE, :features].astype(F32)
        gain = pieces[0:1] + pieces[1:2] + pieces[2:3]
        normed = (wide * gain).astype(BF16)
        total = total + dot(normed, ref[:features, :], ((1,), (0,)))
        squares = squares + jnp.sum(wide * wide, axis=-1, keepdims=True)
    at = total.shape[1] - LANES
    tail = in_pieces(with_squares(total[:, at:], squares))
    block = rows // len(out_refs)
    for k, ref in enumerate(out_refs):
        ref[:, :at] = total[k * block : (k + 1) * block, :at].astype(BF16)
        ref[:, at:] = tail[k * block : (k + 1) * block]


def project_later(blocks, stream, own, other):
    rows = stream.shape[0] // 2
    out = jax.ShapeDtypeStruct((rows // blocks, own.shape[1]), BF16)
    return pl.pallas_call(
        later_kernel,
        out_shape=[out] * blocks,
        in_specs=[VMEM_SPEC] * 3,
        out_specs=[VMEM_SPEC] * blocks,
        compiler_params=params(8),
        cost_estimate=long_cost(),
    )(stream, own, other)


def mix_kernel(
    layer, given, *refs
):
    mix_body(layer, refs[:given], *refs[given:])


def mix_body(
    layer, parts, lengths_ref, taps_ref, bias_ref, alog_ref, skip_ref, gain_ref, past_ref, state_ref,
    mixed_ref, scaled_ref, keys_ref, decay_ref, current_ref,
):
    state, past_ref = state_ref.at[layer], past_ref.at[layer]
    seqs = parts[0].shape[0]
    heads, head_dim, width_n = state.shape[1:]
    width_x = heads * head_dim
    conv = width_x + 2 * width_n
    total = sum(part[...].astype(F32) for part in parts)
    extras = total[:, conv + width_x :]
    extras = extras + pltpu.roll(extras, LANES - PIECE, 1)
    inverse = lax.rsqrt(extras[:, PIECE // 2 : PIECE // 2 + 1] / D + EPSILON)
    current = (total[:, :conv] * inverse).astype(BF16)
    gating = (total[:, conv : conv + width_x] * inverse).astype(BF16).astype(F32)
    current_ref[...] = current

    row = iota((seqs, 1), 0)
    lengths = as_column(lengths_ref)
    taps = taps_ref[layer].astype(F32)
    summed = current.astype(F32) * taps[CONV_W - 1 : CONV_W]
    for j in range(CONV_W - 1):
        past = past_ref[j].astype(F32)
        summed = summed + jnp.where(lengths + j >= CONV_W, past, 0.0) * taps[j : j + 1]
    activated = summed / (1.0 + jnp.exp(-summed))
    head_in = activated[:, :width_x]
    write_keys = activated[:, width_x : width_x + width_n]
    read_keys = activated[:, width_x + width_n :]

    raw = extras[:, :heads] * inverse + bias_ref[layer : layer + 1, :]
    step = jnp.maximum(raw, 0.0) + jnp.log1p(jnp.exp(-jnp.abs(raw)))
    decay = jnp.exp(-jnp.exp(alog_ref[layer : layer + 1, :]) * step)
    decay = jnp.where(lengths >= 2, decay, 0.0)
    lane = iota((seqs, width_x), 1)

    def spread(value):
        out = value[:, 0:1]
        for h in range(1, heads):
            out = jnp.where(lane >= h * head_dim, value[:, h : h + 1], out)
        return out

    scaled = spread(step) * head_in
    scaled_ref[...] = scaled
    keys_ref[...] = write_keys
    decay_ref[...] = decay

    high, low = split(read_keys)
    left = jnp.concatenate(
        [jnp.concatenate([high, high], axis=1), jnp.concatenate([low, jnp.zeros_like(low)], axis=1)], axis=0
    )
    seen = jnp.zeros((seqs, width_x), F32)
    for s in range(seqs):
        old_high, old_low = split(state[s].reshape(width_x, width_n))
        both = dot(left, jnp.concatenate([old_high, old_low], axis=1), ((1,), (1,)))
        seen = jnp.where(row == s, both[:seqs] + both[seqs:], seen)
    pair = jnp.sum(write_keys * read_keys, axis=-1, keepdims=True)
    readout = spread(decay) * seen + scaled * pair + spread(skip_ref[layer : layer + 1, :]) * head_in
    gated = readout * (gating / (1.0 + jnp.exp(-gating)))
    mean = jnp.mean(gated * gated, axis=-1, keepdims=True)
    mixed = (gated * lax.rsqrt(mean + EPSILON) * gain_ref[layer : layer + 1, :]).astype(BF16)
    mixed_ref[...] = mixed


def mix(layer, parts, lengths, taps, bias, alog, skip, gain, past, state):
    seqs = parts[0].shape[-2]
    heads, head_dim, width_n = state.shape[2:]
    width_x = heads * head_dim
    shapes = (
        jax.ShapeDtypeStruct((seqs, width_x), BF16),
        jax.ShapeDtypeStruct((seqs, width_x), F32),
        jax.ShapeDtypeStruct((seqs, width_n), F32),
        jax.ShapeDtypeStruct((seqs, heads), F32),
        jax.ShapeDtypeStruct((seqs, width_x + 2 * width_n), BF16),
    )
    return pl.pallas_call(
        functools.partial(mix_kernel, layer, len(parts)),
        out_shape=shapes,
        in_specs=[*[VMEM_SPEC] * (len(parts) + 8)],
        out_specs=[VMEM_SPEC] * len(shapes),
        compiler_params=params(12),
    )(*parts, lengths, taps, bias, alog, skip, gain, past, state)


def output_kernel(layer, given, *refs):
    mixed = jnp.concatenate([ref[...] for ref in refs[:given]], axis=0)
    own_ref, other_ref, out_ref = refs[given:]
    rows = mixed.shape[0]
    for k, ref in enumerate((own_ref, other_ref)):
        out_ref[k * rows : (k + 1) * rows, :] = dot(mixed, ref[layer], ((1,), (0,))).astype(BF16)


def output(layer, mixed, own, other):
    rows = sum(m.shape[0] for m in mixed)
    return pl.pallas_call(
        functools.partial(output_kernel, layer, len(mixed)),
        out_shape=jax.ShapeDtypeStruct((2 * rows, own.shape[2]), BF16),
        in_specs=[VMEM_SPEC] * (len(mixed) + 2),
        out_specs=VMEM_SPEC,
        compiler_params=params(4),
    )(*mixed, own, other)


def add_kernel(block, parts_ref, *refs):
    streams, out_ref = refs[:-1], refs[-1]
    copies, rows, _ = parts_ref.shape
    total = sum(parts_ref[k].astype(F32) for k in range(copies))
    at = lax.axis_index("tp")
    if len(streams) == 1:
        old = streams[0][pl.ds(pl.multiple_of(at * rows, rows), rows), :]
    else:
        half = copies // 2
        group = lax.rem(at, half)
        per = block // rows
        start = block_at(group // per) * block + lax.rem(group, per) * rows
        first, second = streams
        features = out_ref.shape[-1]
        lowest = second.shape[0] - first.shape[0]
        picked = [
            first[pl.ds(pl.multiple_of(start, rows), rows), :],
            second[pl.ds(pl.multiple_of(lowest + start, rows), rows), :features],
        ]
        old = jnp.where(at < half, picked[0], picked[1])
    new = (old.astype(F32) + total).astype(BF16)
    for k in range(copies):
        out_ref[k] = new


def add(block, parts, streams):
    return pl.pallas_call(
        functools.partial(add_kernel, block),
        out_shape=jax.ShapeDtypeStruct(parts.shape, BF16),
        in_specs=[VMEM_SPEC] * (1 + len(streams)),
        out_specs=VMEM_SPEC,
        compiler_params=params(4),
    )(parts, *streams)


def order_kernel(block, own_ref, other_ref, out_ref):
    copies, rows, _ = own_ref.shape
    per = block // rows
    half = copies // 2
    for k in range(half // per):
        index = block_at(k)
        for ref, at in ((own_ref, index), (other_ref, lax.bitwise_xor(index, jnp.int32(1)))):
            value = jnp.concatenate([ref[k * per + s] for s in range(per)], axis=0)
            out_ref[pl.ds(pl.multiple_of(at * block, block), block), :] = value


def order(block, own, other):
    copies, rows, features = own.shape
    return pl.pallas_call(
        functools.partial(order_kernel, block),
        out_shape=jax.ShapeDtypeStruct((copies * rows, features), BF16),
        in_specs=[VMEM_SPEC] * 2,
        out_specs=VMEM_SPEC,
        compiler_params=params(4),
        name="order",
    )(own, other)


def states_kernel(layer, pieces, lengths_ref, past_ref, state_ref, scaled_ref, keys_ref, decay_ref, current_ref, *refs):
    conv_ref, new_ref, columns, conv, new, left = refs[-6:]
    seqs, heads, head_dim, _ = new.shape
    piece = seqs // pieces

    def copy(k):
        rows = pl.ds(k * piece, piece)
        return pltpu.make_async_copy(new.at[rows], new_ref.at[layer, rows], left.at[k])

    scaled = scaled_ref[...]
    rest = jnp.zeros((LANES - seqs, scaled.shape[1]), F32)
    columns[...] = jnp.concatenate([scaled, rest], axis=0).T
    for s in range(seqs):
        for h in range(heads):
            column = columns[h * head_dim : (h + 1) * head_dim, s : s + 1]
            old = decay_ref[s : s + 1, h : h + 1] * state_ref[layer, s, h]
            new[s, h] = old + column * keys_ref[s : s + 1, :]
        if s % piece == 0 and s > 0:
            copy(s // piece - 1).start()
    lengths = as_column(lengths_ref)
    for j in range(1, CONV_W - 1):
        past = past_ref[layer, j].astype(F32)
        conv[j - 1] = jnp.where(lengths + j >= CONV_W, past, 0.0).astype(BF16)
    conv[CONV_W - 2] = current_ref[...]
    copy(pieces - 1).start()
    for k in range(pieces):
        copy(k).wait()
    last = pltpu.make_async_copy(conv, conv_ref.at[layer], left.at[pieces])
    last.start()
    last.wait()


def states(layer, pieces, lengths, past, state, scaled, keys, decay, current, before):
    _, heads, head_dim, _ = state.shape[1:]
    anywhere = pl.BlockSpec(memory_space=pl.ANY)
    inputs = (lengths, past, state, scaled, keys, decay, current)
    return pl.pallas_call(
        functools.partial(states_kernel, layer, pieces),
        out_shape=(jax.ShapeDtypeStruct(past.shape, past.dtype), jax.ShapeDtypeStruct(state.shape, F32)),
        in_specs=[*[VMEM_SPEC] * len(inputs), *[anywhere] * len(before)],
        out_specs=(anywhere, anywhere),
        input_output_aliases={len(inputs) + k: k for k in range(len(before))},
        scratch_shapes=[
            pltpu.VMEM((heads * head_dim, LANES), F32),
            pltpu.VMEM(past.shape[1:], BF16),
            pltpu.VMEM(state.shape[1:], F32),
            pltpu.SemaphoreType.DMA((pieces + 1,)),
        ],
        compiler_params=params(8),
        cost_estimate=pl.CostEstimate(flops=2_000_000_000, bytes_accessed=4 * state.size, transcendentals=0),
    )(*inputs, *before)


def exchange(blocks, axis):
    return lax.all_to_all(blocks, axis, 0, 0, tiled=True)


def body(
    tokens, lengths, norm_gain, w_z, w_x, w_b, w_c, w_dt, conv_weight, dt_bias, a_log, d_skip, out_gain, w_out,
    conv_state, ssm_state,
):
    tp, dp = lax.axis_size("tp"), lax.axis_size("dp")
    if GROUPS != tp or dp & (dp - 1):
        raise ValueError("unexpected mesh")
    local_heads = HEADS // tp
    rows, features = tokens.shape
    block = rows // dp
    layers = w_z.shape[0]
    w_dt = jnp.swapaxes(w_dt, 1, 2)
    past = jnp.swapaxes(conv_state, 1, 2)
    lengths = lengths.reshape(1, -1)
    across = [2 * k for k in range(1, dp // 2)]

    def over_x(blocks):
        return [blocks[0], *(swapped(b, mask) for b, mask in zip(blocks[1:], across))]

    parts, own_packs = project_first(
        local_heads, block, dp // 2, tokens, norm_gain, w_x, w_b, w_c, w_z, w_dt
    )
    other_packs = [swapped(pack, 1) for pack in own_packs]
    parts = over_x(parts)
    other_out = swapped(w_out, 1)
    streams = [tokens, other_packs[0]]
    made = ()
    for layer in range(layers):
        last = layer == layers - 1
        mixed, *rest = mix(
            layer, parts, lengths, conv_weight, dt_bias, a_log, d_skip, out_gain, past, ssm_state
        )
        mixed = over_x([mixed] * (dp // 2))
        if layer == 0:
            mixed, other_packs = lax.optimization_barrier((mixed, other_packs))
        if last:
            made = states(layer, PIECES, lengths, past, ssm_state, *rest, made)
            mixed, made = lax.optimization_barrier((mixed, made))
        share = output(layer, mixed, w_out, other_out)
        share = exchange(share.reshape(tp, rows // tp, features), "tp")
        new = exchange(add(block, share, streams), "tp")
        if not last:
            streams = [new.reshape(rows, features)]
            parts = project_later(dp // 2, streams[0], own_packs[layer], other_packs[layer])
            parts, rest = lax.optimization_barrier((parts, rest))
            parts = over_x(parts)
            made = states(layer, PIECES, lengths, past, ssm_state, *rest, made)
            parts, made = lax.optimization_barrier((parts, made))
    conv_new, ssm_new = made
    return order(block, new, swapped(new[tp // 2 :], 1)), jnp.swapaxes(conv_new, 1, 2), ssm_new


def solution(mesh):
    by_seq = ("grp", "dp")
    placed = (
        P("grp", "dp"),
        P(by_seq),
        P(None, "dp"),
        P(None, "dp", "tp"),
        P(None, "dp", "tp"),
        P(None, "dp", "tp"),
        P(None, "dp", "tp"),
        P(None, "dp", None),
        P(None, None, "tp"),
        P(None, "tp"),
        P(None, "tp"),
        P(None, "tp"),
        P(None, "tp"),
        P(None, "tp", "dp"),
        P(None, by_seq, None, "tp"),
        P(None, by_seq, "tp", None, None),
    )
    return jax.shard_map(
        body,
        mesh=mesh,
        in_specs=placed,
        out_specs=(P("grp", "dp"), P(None, by_seq, None, "tp"), P(None, by_seq, "tp", None, None)),
        check_vma=False,
    )
```

profile of v0, /device:TPU:40, one launch (start us, length us, event | category | flops | bytes accessed | tf_op | source)
XLA Modules:
  0.0 128.3 jit_solution(13258690267857867316)
XLA Ops:
  0.7 0.8 copy-done.3
  2.1 0.5 project_0.1
  2.8 0.5 collective-permute-start.8
  3.5 0.7 collective-permute-done.arrived_ref
  4.3 1.7 %collective-permute-start.1 = (bf16[16,896]{1,0:T(8,128)(2,1)S(1)}, bf16[16,896]{1,0:T(8,128)(2,1)S(1)}, u32[]{:S(2)}, u32[]{:S(2)}) collective-permute-start(bf16[16,896]{1,0:T(8,128)(2,1)S(1)} %get-tuple-element.56), channel_id=1, source_target_pairs={{0,2},{1,3},{2,0},{3,1},{4,6},{5,7},{6,4},{7,5},{8,10},{9,11},{10,... | collective-permute-start | bytes 86024 | tf_op jit(solution)/shard_map/ppermute | solution.py:71
  6.1 3.0 %collective-permute-start.2 = (bf16[16,896]{1,0:T(8,128)(2,1)S(1)}, bf16[16,896]{1,0:T(8,128)(2,1)S(1)}, u32[]{:S(2)}, u32[]{:S(2)}) collective-permute-start(bf16[16,896]{1,0:T(8,128)(2,1)S(1)} %get-tuple-element.57), channel_id=1, source_target_pairs={{0,4},{1,5},{2,6},{3,7},{4,0},{5,1},{6,2},{7,3},{8,12},{9,13},{10,... | collective-permute-start | bytes 86024 | tf_op jit(solution)/shard_map/ppermute | solution.py:71
  9.2 2.3 %collective-permute-done.2.refs_2_ = bf16[16,896]{1,0:T(8,128)(2,1)S(1)} collective-permute-done((bf16[16,896]{1,0:T(8,128)(2,1)S(1)}, bf16[16,896]{1,0:T(8,128)(2,1)S(1)}, u32[]{:S(2)}, u32[]{:S(2)}) %collective-permute-start.2) | collective-permute-done | bytes 28704 | tf_op jit(solution)/shard_map/ppermute | solution.py:71
  11.5 2.7 %collective-permute-done.3.refs_3_ = bf16[16,896]{1,0:T(8,128)(2,1)S(1)} collective-permute-done((bf16[16,896]{1,0:T(8,128)(2,1)S(1)}, bf16[16,896]{1,0:T(8,128)(2,1)S(1)}, u32[]{:S(2)}, u32[]{:S(2)}) %collective-permute-start.3) | collective-permute-done | bytes 28704 | tf_op jit(solution)/shard_map/ppermute | solution.py:71
  14.2 0.9 shard_map.175
  15.3 0.9 collective-permute-start.5
  16.2 3.1 %collective-permute-start.4 = (bf16[16,256]{1,0:T(8,128)(2,1)S(1)}, bf16[16,256]{1,0:T(8,128)(2,1)S(1)}, u32[]{:S(2)}, u32[]{:S(2)}) collective-permute-start(bf16[16,256]{1,0:T(8,128)(2,1)S(1)} %get-tuple-element.61.refs_0_), channel_id=1, source_target_pairs={{0,2},{1,3},{2,0},{3,1},{4,6},{5,7},{6,4},{7,5},{8,10},{9,11},{10,... | collective-permute-start | bytes 24584 | tf_op jit(solution)/shard_map/ppermute | solution.py:71
  19.3 0.8 collective-permute-done.6.refs_3_
  20.1 0.4 collective-permute-done.5.refs_2_
  20.5 0.5 collective-permute-done.4.refs_1_
  21.0 0.2 shard_map.176
  21.3 36.8 %all_to_all.20.parts_ref = bf16[16,8,512]{2,1,0:T(8,128)(2,1)S(1)} all-to-all(bf16[16,8,512]{2,1,0:T(8,128)(2,1)S(1)} %bitcast.14), channel_id=1, replica_groups=mesh['grp'=2,'tp'=16,'dp'=8] {'tp'}, dimensions={0} | all-to-all | bytes 262144 | tf_op jit(solution)/shard_map/all_to_all | solution.py:425
  58.1 16.8 %all_to_all.21 = bf16[16,8,512]{2,1,0:T(8,128)(2,1)S(1)} all-to-all(bf16[16,8,512]{2,1,0:T(8,128)(2,1)S(1)} %shard_map.177), channel_id=1, replica_groups=mesh['grp'=2,'tp'=16,'dp'=8] {'tp'}, dimensions={0} | all-to-all | bytes 262144 | tf_op jit(solution)/shard_map/all_to_all | solution.py:425
  75.0 0.4 shard_map.178
  75.4 2.1 %collective-permute-start.9 = (bf16[16,896]{1,0:T(8,128)(2,1)S(1)}, bf16[16,896]{1,0:T(8,128)(2,1)S(1)}, u32[]{:S(2)}, u32[]{:S(2)}) collective-permute-start(bf16[16,896]{1,0:T(8,128)(2,1)S(1)} %get-tuple-element.75), channel_id=1, source_target_pairs={{0,2},{1,3},{2,0},{3,1},{4,6},{5,7},{6,4},{7,5},{8,10},{9,11},{10,... | collective-permute-start | bytes 86024 | tf_op jit(solution)/shard_map/ppermute | solution.py:71
  77.5 2.1 %collective-permute-start.10 = (bf16[16,896]{1,0:T(8,128)(2,1)S(1)}, bf16[16,896]{1,0:T(8,128)(2,1)S(1)}, u32[]{:S(2)}, u32[]{:S(2)}) collective-permute-start(bf16[16,896]{1,0:T(8,128)(2,1)S(1)} %get-tuple-element.76), channel_id=1, source_target_pairs={{0,4},{1,5},{2,6},{3,7},{4,0},{5,1},{6,2},{7,3},{8,12},{9,13},{10,... | collective-permute-start | bytes 86024 | tf_op jit(solution)/shard_map/ppermute | solution.py:71
  79.6 0.7 collective-permute-start.11
  80.3 2.4 %shard_map.179 = (bf16[2,3,16,512]{3,2,1,0:T(8,128)(2,1)}, f32[2,16,4,64,128]{4,3,2,1,0:T(8,128)}) custom-call(s32[1,16]{1,0:T(1,128)S(1)} %bitcast.17, bf16[2,3,16,512]{3,2,1,0:T(8,128)(2,1)S(1)} %bitcast.8, f32[2,16,4,64,128]{4,3,2,1,0:T(8,128)S(1)} %copy-done, f32[16,256]{1,0:T(8,128)S(1)} %get-tuple-element.78.scaled_ref, ...), custom_call_target="tpu_custom_call" | custom-call | flops 2000000000 | bytes 4194304 | tf_op jit(solution)/shard_map/pallas_call | solution.py:407
  82.9 1.8 %collective-permute-done.11.refs_3_ = bf16[16,896]{1,0:T(8,128)(2,1)S(1)} collective-permute-done((bf16[16,896]{1,0:T(8,128)(2,1)S(1)}, bf16[16,896]{1,0:T(8,128)(2,1)S(1)}, u32[]{:S(2)}, u32[]{:S(2)}) %collective-permute-start.11) | collective-permute-done | bytes 28704 | tf_op jit(solution)/shard_map/ppermute | solution.py:71
  84.7 0.9 shard_map.180
  85.6 0.9 collective-permute-start.14
  86.6 3.2 %collective-permute-start.12 = (bf16[16,256]{1,0:T(8,128)(2,1)S(1)}, bf16[16,256]{1,0:T(8,128)(2,1)S(1)}, u32[]{:S(2)}, u32[]{:S(2)}) collective-permute-start(bf16[16,256]{1,0:T(8,128)(2,1)S(1)} %get-tuple-element.97.refs_0_), channel_id=1, source_target_pairs={{0,2},{1,3},{2,0},{3,1},{4,6},{5,7},{6,4},{7,5},{8,10},{9,11},{10,... | collective-permute-start | bytes 24584 | tf_op jit(solution)/shard_map/ppermute | solution.py:71
  89.8 2.4 %shard_map.181 = (bf16[2,3,16,512]{3,2,1,0:T(8,128)(2,1)}, f32[2,16,4,64,128]{4,3,2,1,0:T(8,128)}) custom-call(s32[1,16]{1,0:T(1,128)S(1)} %bitcast.19, bf16[2,3,16,512]{3,2,1,0:T(8,128)(2,1)S(1)} %bitcast.10, f32[2,16,4,64,128]{4,3,2,1,0:T(8,128)S(1)} %copy-done, ...), custom_call_target="tpu_custom_call", output_to_operand_aliasing={{0}: (7, {}), {1}: (8, {})} | custom-call | flops 2000000000 | bytes 4194304 | tf_op jit(solution)/shard_map/pallas_call | solution.py:407
  92.2 0.2 shard_map.182
  92.4 16.9 %all_to_all.22.parts_ref = bf16[16,8,512]{2,1,0:T(8,128)(2,1)S(1)} all-to-all(bf16[16,8,512]{2,1,0:T(8,128)(2,1)S(1)} %bitcast.13), channel_id=1, replica_groups=mesh['grp'=2,'tp'=16,'dp'=8] {'tp'}, dimensions={0} | all-to-all | bytes 262144 | tf_op jit(solution)/shard_map/all_to_all | solution.py:425
  109.4 17.0 %all_to_all.23.own_ref = bf16[16,8,512]{2,1,0:T(8,128)(2,1)S(1)} all-to-all(bf16[16,8,512]{2,1,0:T(8,128)(2,1)S(1)} %shard_map.183), channel_id=1, replica_groups=mesh['grp'=2,'tp'=16,'dp'=8] {'tp'}, dimensions={0} | all-to-all | bytes 262144 | tf_op jit(solution)/shard_map/all_to_all | solution.py:425
  126.3 1.2 collective-permute-done.15.other_ref
  127.6 0.7 order.1
  (50 shorter events, 1.7 us)
Async XLA Ops:
  0.6 0.9 copy-start.3
  0.6 1.0 copy-start.8
  0.7 1.1 copy-start.7
  0.7 1.1 copy-start.6
  0.7 1.3 %copy-start.4 = (bf16[2,512,256]{2,1,0:T(8,128)(2,1)S(1)}, bf16[2,512,256]{2,1,0:T(8,128)(2,1)}, u32[]{:S(2)}) copy-start(bf16[2,512,256]{2,1,0:T(8,128)(2,1)} %wx_ref.1) | copy-start | bytes 1572868
  0.7 1.5 %copy-start.5 = (bf16[2,512,256]{2,1,0:T(8,128)(2,1)S(1)}, bf16[2,512,256]{2,1,0:T(8,128)(2,1)}, u32[]{:S(2)}) copy-start(bf16[2,512,256]{2,1,0:T(8,128)(2,1)} %wz_ref.1) | copy-start | bytes 1572868
  0.7 1.4 %copy-start.12 = (f32[2,512]{1,0:T(2,128)S(1)}, f32[2,512]{1,0:T(2,128)}, u32[]{:S(2)}) copy-start(f32[2,512]{1,0:T(2,128)} %gain_ref.1) | copy-start | bytes 12292
  0.7 2.1 %copy-start.1 = (bf16[2,256,512]{2,1,0:T(8,128)(2,1)S(1)}, bf16[2,256,512]{2,1,0:T(8,128)(2,1)}, u32[]{:S(2)}) copy-start(bf16[2,256,512]{2,1,0:T(8,128)(2,1)} %refs_4_.3) | copy-start | bytes 1572868
  2.7 1.4 %collective-permute-start = (bf16[64,896]{1,0:T(8,128)(2,1)S(1)}, bf16[64,896]{1,0:T(8,128)(2,1)S(1)}, u32[]{:S(2)}, u32[]{:S(2)}) collective-permute-start(bf16[64,896]{1,0:T(8,128)(2,1)S(1)} %get-tuple-element.54), channel_id=1, source_target_pairs={{0,1},{1,0},{2,3},{3,2},{4,5},{5,4},{6,7},{7,6},{8,9},{9,8},{10,11... | collective-permute-start | bytes 344072 | tf_op jit(solution)/shard_map/ppermute | solution.py:71
  2.8 18.2 %collective-permute-start.8 = (bf16[2,256,512]{2,1,0:T(8,128)(2,1)S(1)}, bf16[2,256,512]{2,1,0:T(8,128)(2,1)S(1)}, u32[]{:S(2)}, u32[]{:S(2)}) collective-permute-start(bf16[2,256,512]{2,1,0:T(8,128)(2,1)S(1)} %copy-done.1), channel_id=1, source_target_pairs={{0,1},{1,0},{2,3},{3,2},{4,5},{5,4},{6,7},{7,6},{8,9},{9,8},{10,11... | collective-permute-start | bytes 1572872 | tf_op jit(solution)/shard_map/ppermute | solution.py:71
  3.3 17.7 %collective-permute-start.7 = (bf16[656,896]{1,0:T(8,128)(2,1)S(1)}, bf16[656,896]{1,0:T(8,128)(2,1)S(1)}, u32[]{:S(2)}, u32[]{:S(2)}) collective-permute-start(bf16[656,896]{1,0:T(8,128)(2,1)S(1)} %get-tuple-element.60.own_ref), channel_id=1, source_target_pairs={{0,1},{1,0},{2,3},{3,2},{4,5},{5,4},{6,7},{7,6},{8,9},{9,8},{10,11... | collective-permute-start | bytes 3526664 | tf_op jit(solution)/shard_map/ppermute | solution.py:71
  4.1 10.1 %copy-start = (f32[2,16,4,64,128]{4,3,2,1,0:T(8,128)S(1)}, f32[2,16,4,64,128]{4,3,2,1,0:T(8,128)}, u32[]{:S(2)}) copy-start(f32[2,16,4,64,128]{4,3,2,1,0:T(8,128)} %state_ref.3) | copy-start | bytes 12582916
  4.1 10.1 %copy-start.2 = (bf16[2,16,3,512]{3,1,2,0:T(8,128)(2,1)S(1)}, bf16[2,16,3,512]{3,1,2,0:T(8,128)(2,1)}, u32[]{:S(2)}) copy-start(bf16[2,16,3,512]{3,1,2,0:T(8,128)(2,1)} %param.30) | copy-start | bytes 294916
  4.1 10.1 %copy-start.9 = (bf16[2,4,512]{2,1,0:T(4,128)(2,1)S(1)}, bf16[2,4,512]{2,1,0:T(4,128)(2,1)}, u32[]{:S(2)}) copy-start(bf16[2,4,512]{2,1,0:T(4,128)(2,1)} %refs_5_.3) | copy-start | bytes 24580
  4.1 10.1 %copy-start.10 = (f32[2,256]{1,0:T(2,128)S(1)}, f32[2,256]{1,0:T(2,128)}, u32[]{:S(2)}) copy-start(f32[2,256]{1,0:T(2,128)} %refs_9_.3) | copy-start | bytes 6148
  4.1 10.1 %copy-start.11 = (s32[16]{0:T(128)S(1)}, s32[16]{0:T(128)}, u32[]{:S(2)}) copy-start(s32[16]{0:T(128)} %param.17) | copy-start | bytes 196
  4.1 10.1 %copy-start.13 = (f32[2,4]{1,0:T(2,128)S(1)}, f32[2,4]{1,0:T(2,128)}, u32[]{:S(2)}) copy-start(f32[2,4]{1,0:T(2,128)} %refs_6_.3) | copy-start | bytes 100
  4.2 10.1 %copy-start.14 = (f32[2,4]{1,0:T(2,128)S(1)}, f32[2,4]{1,0:T(2,128)}, u32[]{:S(2)}) copy-start(f32[2,4]{1,0:T(2,128)} %refs_7_.3) | copy-start | bytes 100
  4.2 10.1 %copy-start.15 = (f32[2,4]{1,0:T(2,128)S(1)}, f32[2,4]{1,0:T(2,128)}, u32[]{:S(2)}) copy-start(f32[2,4]{1,0:T(2,128)} %refs_8_.3) | copy-start | bytes 100
  4.3 4.8 %collective-permute-start.1 = (bf16[16,896]{1,0:T(8,128)(2,1)S(1)}, bf16[16,896]{1,0:T(8,128)(2,1)S(1)}, u32[]{:S(2)}, u32[]{:S(2)}) collective-permute-start(bf16[16,896]{1,0:T(8,128)(2,1)S(1)} %get-tuple-element.56), channel_id=1, source_target_pairs={{0,2},{1,3},{2,0},{3,1},{4,6},{5,7},{6,4},{7,5},{8,10},{9,11},{10,... | collective-permute-start | bytes 86024 | tf_op jit(solution)/shard_map/ppermute | solution.py:71
  6.1 5.4 %collective-permute-start.2 = (bf16[16,896]{1,0:T(8,128)(2,1)S(1)}, bf16[16,896]{1,0:T(8,128)(2,1)S(1)}, u32[]{:S(2)}, u32[]{:S(2)}) collective-permute-start(bf16[16,896]{1,0:T(8,128)(2,1)S(1)} %get-tuple-element.57), channel_id=1, source_target_pairs={{0,4},{1,5},{2,6},{3,7},{4,0},{5,1},{6,2},{7,3},{8,12},{9,13},{10,... | collective-permute-start | bytes 86024 | tf_op jit(solution)/shard_map/ppermute | solution.py:71
  9.1 5.1 %collective-permute-start.3 = (bf16[16,896]{1,0:T(8,128)(2,1)S(1)}, bf16[16,896]{1,0:T(8,128)(2,1)S(1)}, u32[]{:S(2)}, u32[]{:S(2)}) collective-permute-start(bf16[16,896]{1,0:T(8,128)(2,1)S(1)} %get-tuple-element.58), channel_id=1, source_target_pairs={{0,6},{1,7},{2,4},{3,5},{4,2},{5,3},{6,0},{7,1},{8,14},{9,15},{10,... | collective-permute-start | bytes 86024 | tf_op jit(solution)/shard_map/ppermute | solution.py:71
  15.1 5.0 %collective-permute-start.6 = (bf16[16,256]{1,0:T(8,128)(2,1)S(1)}, bf16[16,256]{1,0:T(8,128)(2,1)S(1)}, u32[]{:S(2)}, u32[]{:S(2)}) collective-permute-start(bf16[16,256]{1,0:T(8,128)(2,1)S(1)} %get-tuple-element.61.refs_0_), channel_id=1, source_target_pairs={{0,6},{1,7},{2,4},{3,5},{4,2},{5,3},{6,0},{7,1},{8,14},{9,15},{10,... | collective-permute-start | bytes 24584 | tf_op jit(solution)/shard_map/ppermute | solution.py:71
  15.3 5.2 %collective-permute-start.5 = (bf16[16,256]{1,0:T(8,128)(2,1)S(1)}, bf16[16,256]{1,0:T(8,128)(2,1)S(1)}, u32[]{:S(2)}, u32[]{:S(2)}) collective-permute-start(bf16[16,256]{1,0:T(8,128)(2,1)S(1)} %get-tuple-element.61.refs_0_), channel_id=1, source_target_pairs={{0,4},{1,5},{2,6},{3,7},{4,0},{5,1},{6,2},{7,3},{8,12},{9,13},{10,... | collective-permute-start | bytes 24584 | tf_op jit(solution)/shard_map/ppermute | solution.py:71
  16.2 4.9 %collective-permute-start.4 = (bf16[16,256]{1,0:T(8,128)(2,1)S(1)}, bf16[16,256]{1,0:T(8,128)(2,1)S(1)}, u32[]{:S(2)}, u32[]{:S(2)}) collective-permute-start(bf16[16,256]{1,0:T(8,128)(2,1)S(1)} %get-tuple-element.61.refs_0_), channel_id=1, source_target_pairs={{0,2},{1,3},{2,0},{3,1},{4,6},{5,7},{6,4},{7,5},{8,10},{9,11},{10,... | collective-permute-start | bytes 24584 | tf_op jit(solution)/shard_map/ppermute | solution.py:71
  75.4 7.3 %collective-permute-start.9 = (bf16[16,896]{1,0:T(8,128)(2,1)S(1)}, bf16[16,896]{1,0:T(8,128)(2,1)S(1)}, u32[]{:S(2)}, u32[]{:S(2)}) collective-permute-start(bf16[16,896]{1,0:T(8,128)(2,1)S(1)} %get-tuple-element.75), channel_id=1, source_target_pairs={{0,2},{1,3},{2,0},{3,1},{4,6},{5,7},{6,4},{7,5},{8,10},{9,11},{10,... | collective-permute-start | bytes 86024 | tf_op jit(solution)/shard_map/ppermute | solution.py:71
  77.5 5.4 %collective-permute-start.10 = (bf16[16,896]{1,0:T(8,128)(2,1)S(1)}, bf16[16,896]{1,0:T(8,128)(2,1)S(1)}, u32[]{:S(2)}, u32[]{:S(2)}) collective-permute-start(bf16[16,896]{1,0:T(8,128)(2,1)S(1)} %get-tuple-element.76), channel_id=1, source_target_pairs={{0,4},{1,5},{2,6},{3,7},{4,0},{5,1},{6,2},{7,3},{8,12},{9,13},{10,... | collective-permute-start | bytes 86024 | tf_op jit(solution)/shard_map/ppermute | solution.py:71
  79.6 5.1 %collective-permute-start.11 = (bf16[16,896]{1,0:T(8,128)(2,1)S(1)}, bf16[16,896]{1,0:T(8,128)(2,1)S(1)}, u32[]{:S(2)}, u32[]{:S(2)}) collective-permute-start(bf16[16,896]{1,0:T(8,128)(2,1)S(1)} %get-tuple-element.77), channel_id=1, source_target_pairs={{0,6},{1,7},{2,4},{3,5},{4,2},{5,3},{6,0},{7,1},{8,14},{9,15},{10,... | collective-permute-start | bytes 86024 | tf_op jit(solution)/shard_map/ppermute | solution.py:71
  85.6 6.6 %collective-permute-start.14 = (bf16[16,256]{1,0:T(8,128)(2,1)S(1)}, bf16[16,256]{1,0:T(8,128)(2,1)S(1)}, u32[]{:S(2)}, u32[]{:S(2)}) collective-permute-start(bf16[16,256]{1,0:T(8,128)(2,1)S(1)} %get-tuple-element.97.refs_0_), channel_id=1, source_target_pairs={{0,6},{1,7},{2,4},{3,5},{4,2},{5,3},{6,0},{7,1},{8,14},{9,15},{10,... | collective-permute-start | bytes 24584 | tf_op jit(solution)/shard_map/ppermute | solution.py:71
  86.4 5.8 %collective-permute-start.13 = (bf16[16,256]{1,0:T(8,128)(2,1)S(1)}, bf16[16,256]{1,0:T(8,128)(2,1)S(1)}, u32[]{:S(2)}, u32[]{:S(2)}) collective-permute-start(bf16[16,256]{1,0:T(8,128)(2,1)S(1)} %get-tuple-element.97.refs_0_), channel_id=1, source_target_pairs={{0,4},{1,5},{2,6},{3,7},{4,0},{5,1},{6,2},{7,3},{8,12},{9,13},{10,... | collective-permute-start | bytes 24584 | tf_op jit(solution)/shard_map/ppermute | solution.py:71
  86.6 5.6 %collective-permute-start.12 = (bf16[16,256]{1,0:T(8,128)(2,1)S(1)}, bf16[16,256]{1,0:T(8,128)(2,1)S(1)}, u32[]{:S(2)}, u32[]{:S(2)}) collective-permute-start(bf16[16,256]{1,0:T(8,128)(2,1)S(1)} %get-tuple-element.97.refs_0_), channel_id=1, source_target_pairs={{0,2},{1,3},{2,0},{3,1},{4,6},{5,7},{6,4},{7,5},{8,10},{9,11},{10,... | collective-permute-start | bytes 24584 | tf_op jit(solution)/shard_map/ppermute | solution.py:71
  126.3 1.3 collective-permute-start.15
where the time goes:
time: 130 us; the launch traced here: 128 us
  blocking collectives  87.5 us (67%)
  starting transfers between devices  19 us (15%)
  waiting for transfers between devices  10.5 us (8%)
  Pallas kernels  8.8 us (7%)
  local copies, waits for them, and re-layouts  1.48 us (1%)
    all_to_all x4, blocking collectives, exchange(): return lax.all_to_all(blocks, axis, 0, 0, tiled=True)  87.5 us
    ppermute x16, starting transfers between devices, swapped(): return lax.ppermute(value, 'dp', pairs)  19 us
    ppermute x16, waiting for transfers between devices, swapped(): return lax.ppermute(value, 'dp', pairs)  10.5 us
    pallas_call x2, Pallas kernels, states(): pl.pallas_call(functools.partial(states_kernel, layer, pieces), out_shape...  4.78 us
  transfers between devices with their start and end apart: 16, of which 9 were waited for; matrix products, arithmetic and copies ran while one was open for 0% of the time, Pallas kernels for 5%

commit v1 on v0

--- a/solution.py
+++ b/solution.py
@@ -92,30 +92,37 @@
     return lax.bitwise_xor(at // 2, jnp.int32(k)) * 2 + at % 2
 
 
-def first_kernel(local_heads, block, x_ref, gain_ref, wx_ref, wb_ref, wc_ref, wz_ref, wdt_ref, _, own_ref, other_ref, *packs):
-    rows, features = x_ref.shape
-    blocks = [block_at(k) for k in range(rows // block // 2)]
-    blocks += [lax.bitwise_xor(b, jnp.int32(1)) for b in blocks]
+def first_rows(local_heads, block, away, x_ref, gain_ref, weights, wdt_ref, out_ref):
+    half = x_ref.shape[0] // 2
+    blocks = [lax.bitwise_xor(block_at(k), jnp.int32(away)) for k in range(half // block)]
     tokens = [x_ref[pl.ds(pl.multiple_of(b * block, block), block), :] for b in blocks]
     wide = jnp.concatenate(tokens, axis=0).astype(F32)
     normed = (wide * gain_ref[0:1, :]).astype(BF16)
-    half = rows // 2
     at = 0
-    for ref in (wx_ref, wb_ref, wc_ref, wz_ref):
+    for ref in weights:
         width = ref.shape[-1]
-        part = dot(normed, ref[0], ((1,), (0,)))
-        own_ref[:, at : at + width] = part[:half]
-        other_ref[:, at : at + width] = part[half:].astype(BF16)
+        out_ref[:, at : at + width] = dot(normed, ref[0], ((1,), (0,))).astype(out_ref.dtype)
         at += width
     chosen = chosen_heads(wdt_ref.shape[1], local_heads)
     steps = dot(wdt_ref[0], chosen, ((0,), (1,))).astype(BF16)
     squares = jnp.sum(wide * wide, axis=-1, keepdims=True)
     extras = with_squares(dot(normed, steps, ((1,), (0,))), squares)
-    own_ref[:, at:] = extras[:half]
-    other_ref[:, at:] = in_pieces(extras[half:])
+    out_ref[:, at:] = in_pieces(extras) if away else extras
+
+
+def away_kernel(local_heads, block, x_ref, gain_ref, wx_ref, wb_ref, wc_ref, wz_ref, wdt_ref, _, out_ref):
+    first_rows(local_heads, block, 1, x_ref, gain_ref, (wx_ref, wb_ref, wc_ref, wz_ref), wdt_ref, out_ref)
+
+
+def home_kernel(local_heads, block, x_ref, gain_ref, wx_ref, wb_ref, wc_ref, wz_ref, wdt_ref, own_ref, *packs):
+    weights = (wx_ref, wb_ref, wc_ref, wz_ref)
+    first_rows(local_heads, block, 0, x_ref, gain_ref, weights, wdt_ref, own_ref)
+    features = x_ref.shape[1]
+    at = own_ref.shape[1] - LANES
+    chosen = chosen_heads(wdt_ref.shape[1], local_heads)
     for layer, pack in enumerate(packs, 1):
         first = 0
-        for ref in (wx_ref, wb_ref, wc_ref, wz_ref):
+        for ref in weights:
             pack[:features, first : first + ref.shape[-1]] = ref[layer]
             first += ref.shape[-1]
         pack[:features, at:] = dot(wdt_ref[layer], chosen, ((0,), (1,))).astype(BF16)
@@ -149,14 +156,23 @@
     own = jax.ShapeDtypeStruct((rows // 2, width), F32)
     other = jax.ShapeDtypeStruct((rows // 2, width), BF16)
     packs = [jax.ShapeDtypeStruct((features + PIECE + rows, width), BF16)] * (w_z.shape[0] - 1)
-    inputs = [stream, norm_gain, w_x, w_b, w_c, w_z, w_dt, gate()]
-    own, other, *packed = pl.pallas_call(
-        functools.partial(first_kernel, local_heads, block),
-        out_shape=(own, other, *packs),
+    inputs = [stream, norm_gain, w_x, w_b, w_c, w_z, w_dt]
+    other = pl.pallas_call(
+        functools.partial(away_kernel, local_heads, block),
+        out_shape=other,
+        in_specs=[VMEM_SPEC] * (1 + len(inputs)),
+        out_specs=VMEM_SPEC,
+        compiler_params=params(8),
+        name="project_away",
+    )(*inputs, gate())
+    own, *packed = pl.pallas_call(
+        functools.partial(home_kernel, local_heads, block),
+        out_shape=(own, *packs),
         in_specs=[VMEM_SPEC] * len(inputs),
-        out_specs=[VMEM_SPEC] * (2 + len(packs)),
+        out_specs=[VMEM_SPEC] * (1 + len(packs)),
         compiler_params=params(8),
-        name="project_0",
+        cost_estimate=pl.CostEstimate(flops=200_000_000, bytes_accessed=2_000_000, transcendentals=0),
+        name="project_home",
     )(*inputs)
     arrived = swapped(other, 1)
     parts = pl.pallas_call(
@@ -212,10 +228,11 @@
     layer, parts, lengths_ref, taps_ref, bias_ref, alog_ref, skip_ref, gain_ref, past_ref, state_ref,
     mixed_ref, scaled_ref, keys_ref, decay_ref, current_ref,
 ):
-    state, past_ref = state_ref.at[layer], past_ref.at[layer]
+    past_ref = past_ref.at[layer]
     seqs = parts[0].shape[0]
-    heads, head_dim, width_n = state.shape[1:]
-    width_x = heads * head_dim
+    heads = bias_ref.shape[1]
+    width_x, width_n = state_ref.shape[2], state_ref.shape[3] // 2
+    head_dim = width_x // heads
     conv = width_x + 2 * width_n
     total = sum(part[...].astype(F32) for part in parts)
     extras = total[:, conv + width_x :]
@@ -260,8 +277,7 @@
     )
     seen = jnp.zeros((seqs, width_x), F32)
     for s in range(seqs):
-        old_high, old_low = split(state[s].reshape(width_x, width_n))
-        both = dot(left, jnp.concatenate([old_high, old_low], axis=1), ((1,), (1,)))
+        both = dot(left, state_ref[layer, s], ((1,), (1,)))
         seen = jnp.where(row == s, both[:seqs] + both[seqs:], seen)
     pair = jnp.sum(write_keys * read_keys, axis=-1, keepdims=True)
     readout = spread(decay) * seen + scaled * pair + spread(skip_ref[layer : layer + 1, :]) * head_in
@@ -273,8 +289,7 @@
 
 def mix(layer, parts, lengths, taps, bias, alog, skip, gain, past, state):
     seqs = parts[0].shape[-2]
-    heads, head_dim, width_n = state.shape[2:]
-    width_x = heads * head_dim
+    heads, width_x, width_n = bias.shape[1], state.shape[2], state.shape[3] // 2
     shapes = (
         jax.ShapeDtypeStruct((seqs, width_x), BF16),
         jax.ShapeDtypeStruct((seqs, width_x), F32),
@@ -368,6 +383,28 @@
     )(own, other)
 
 
+def prepare_kernel(_, state_ref, out_ref):
+    layers, seqs, heads, head_dim, width_n = state_ref.shape
+    for layer in range(layers):
+        for s in range(seqs):
+            high, low = split(state_ref[layer, s].reshape(heads * head_dim, width_n))
+            out_ref[layer, s, :, :width_n] = high
+            out_ref[layer, s, :, width_n:] = low
+
+
+def prepare(after, state):
+    layers, seqs, heads, head_dim, width_n = state.shape
+    return pl.pallas_call(
+        prepare_kernel,
+        out_shape=jax.ShapeDtypeStruct((layers, seqs, heads * head_dim, 2 * width_n), BF16),
+        in_specs=[VMEM_SPEC] * 2,
+        out_specs=VMEM_SPEC,
+        compiler_params=params(12),
+        cost_estimate=pl.CostEstimate(flops=500_000_000, bytes_accessed=2 * state.size, transcendentals=0),
+        name="prepare",
+    )(after, state)
+
+
 def states_kernel(layer, pieces, lengths_ref, past_ref, state_ref, scaled_ref, keys_ref, decay_ref, current_ref, *refs):
     conv_ref, new_ref, columns, conv, new, left = refs[-6:]
     seqs, heads, head_dim, _ = new.shape
@@ -448,6 +485,7 @@
         local_heads, block, dp // 2, tokens, norm_gain, w_x, w_b, w_c, w_z, w_dt
     )
     other_packs = [swapped(pack, 1) for pack in own_packs]
+    pieces = prepare(parts[0], ssm_state)
     parts = over_x(parts)
     other_out = swapped(w_out, 1)
     streams = [tokens, other_packs[0]]
@@ -455,7 +493,7 @@
     for layer in range(layers):
         last = layer == layers - 1
         mixed, *rest = mix(
-            layer, parts, lengths, conv_weight, dt_bias, a_log, d_skip, out_gain, past, ssm_state
+            layer, parts, lengths, conv_weight, dt_bias, a_log, d_skip, out_gain, past, pieces
         )
         mixed = over_x([mixed] * (dp // 2))
         if layer == 0:

time: 130 us -> 130 us (level)
    ppermute x16, waiting for transfers between devices: 10.5 us -> 9.25 us  [swapped(): return lax.ppermute(value, 'dp', pairs)]
  transfers between devices with their start and end apart: 16 -> 16, of which waited for: 9 -> 8; matrix products, arithmetic and copies ran while one was open for 0% -> 0% of each run, Pallas kernels for 5% -> 5%
where the time goes in v1:
time: 130 us; the launch traced here: 128 us
  blocking collectives  87.6 us (67%)
  starting transfers between devices  19.2 us (15%)
  Pallas kernels  9.87 us (8%)
  waiting for transfers between devices  9.25 us (7%)
  local copies, waits for them, and re-layouts  1.44 us (1%)
    all_to_all x4, blocking collectives, exchange(): return lax.all_to_all(blocks, axis, 0, 0, tiled=True)  87.6 us
    ppermute x16, starting transfers between devices, swapped(): return lax.ppermute(value, 'dp', pairs)  19.2 us
    ppermute x16, waiting for transfers between devices, swapped(): return lax.ppermute(value, 'dp', pairs)  9.25 us
    pallas_call x2, Pallas kernels, states(): pl.pallas_call(functools.partial(states_kernel, layer, pieces), out_shape...  4.79 us
  transfers between devices with their start and end apart: 16, of which 8 were waited for; matrix products, arithmetic and copies ran while one was open for 0% of the time, Pallas kernels for 5%

profile of v1, /device:TPU:40, one launch (start us, length us, event | category | flops | bytes accessed | tf_op | source)
XLA Modules:
  0.0 128.3 jit_solution(5199645023769674397)
XLA Ops:
  0.7 0.8 copy-done.4
  2.1 0.4 project_away.1
  2.7 0.5 collective-permute-start.8
  3.2 0.5 project_home.1
  3.7 0.3 collective-permute-start.7
  4.1 1.7 %collective-permute-start.1 = (bf16[16,896]{1,0:T(8,128)(2,1)S(1)}, bf16[16,896]{1,0:T(8,128)(2,1)S(1)}, u32[]{:S(2)}, u32[]{:S(2)}) collective-permute-start(bf16[16,896]{1,0:T(8,128)(2,1)S(1)} %get-tuple-element.54), channel_id=1, source_target_pairs={{0,2},{1,3},{2,0},{3,1},{4,6},{5,7},{6,4},{7,5},{8,10},{9,11},{10,... | collective-permute-start | bytes 86024 | tf_op jit(solution)/shard_map/ppermute | solution.py:71
  5.9 3.0 %collective-permute-start.2 = (bf16[16,896]{1,0:T(8,128)(2,1)S(1)}, bf16[16,896]{1,0:T(8,128)(2,1)S(1)}, u32[]{:S(2)}, u32[]{:S(2)}) collective-permute-start(bf16[16,896]{1,0:T(8,128)(2,1)S(1)} %get-tuple-element.55), channel_id=1, source_target_pairs={{0,4},{1,5},{2,6},{3,7},{4,0},{5,1},{6,2},{7,3},{8,12},{9,13},{10,... | collective-permute-start | bytes 86024 | tf_op jit(solution)/shard_map/ppermute | solution.py:71
  9.0 0.7 prepare.1.refs_11_
  9.7 1.5 %collective-permute-done.2.refs_2_ = bf16[16,896]{1,0:T(8,128)(2,1)S(1)} collective-permute-done((bf16[16,896]{1,0:T(8,128)(2,1)S(1)}, bf16[16,896]{1,0:T(8,128)(2,1)S(1)}, u32[]{:S(2)}, u32[]{:S(2)}) %collective-permute-start.2) | collective-permute-done | bytes 28704 | tf_op jit(solution)/shard_map/ppermute | solution.py:71
  11.3 2.7 %collective-permute-done.3.refs_3_ = bf16[16,896]{1,0:T(8,128)(2,1)S(1)} collective-permute-done((bf16[16,896]{1,0:T(8,128)(2,1)S(1)}, bf16[16,896]{1,0:T(8,128)(2,1)S(1)}, u32[]{:S(2)}, u32[]{:S(2)}) %collective-permute-start.3) | collective-permute-done | bytes 28704 | tf_op jit(solution)/shard_map/ppermute | solution.py:71
  14.0 0.9 shard_map.175
  15.1 0.9 collective-permute-start.5
  16.0 3.1 %collective-permute-start.4 = (bf16[16,256]{1,0:T(8,128)(2,1)S(1)}, bf16[16,256]{1,0:T(8,128)(2,1)S(1)}, u32[]{:S(2)}, u32[]{:S(2)}) collective-permute-start(bf16[16,256]{1,0:T(8,128)(2,1)S(1)} %get-tuple-element.59.refs_0_), channel_id=1, source_target_pairs={{0,2},{1,3},{2,0},{3,1},{4,6},{5,7},{6,4},{7,5},{8,10},{9,11},{10,... | collective-permute-start | bytes 24584 | tf_op jit(solution)/shard_map/ppermute | solution.py:71
  19.1 0.8 collective-permute-done.6.refs_3_
  19.9 0.4 collective-permute-done.5.refs_2_
  20.3 0.5 collective-permute-done.4.refs_1_
  21.0 36.7 %all_to_all.20.parts_ref = bf16[16,8,512]{2,1,0:T(8,128)(2,1)S(1)} all-to-all(bf16[16,8,512]{2,1,0:T(8,128)(2,1)S(1)} %bitcast.14), channel_id=1, replica_groups=mesh['grp'=2,'tp'=16,'dp'=8] {'tp'}, dimensions={0} | all-to-all | bytes 262144 | tf_op jit(solution)/shard_map/all_to_all | solution.py:462
  57.8 17.0 %all_to_all.21 = bf16[16,8,512]{2,1,0:T(8,128)(2,1)S(1)} all-to-all(bf16[16,8,512]{2,1,0:T(8,128)(2,1)S(1)} %shard_map.177), channel_id=1, replica_groups=mesh['grp'=2,'tp'=16,'dp'=8] {'tp'}, dimensions={0} | all-to-all | bytes 262144 | tf_op jit(solution)/shard_map/all_to_all | solution.py:462
  74.8 0.4 shard_map.178
  75.2 2.0 %collective-permute-start.9 = (bf16[16,896]{1,0:T(8,128)(2,1)S(1)}, bf16[16,896]{1,0:T(8,128)(2,1)S(1)}, u32[]{:S(2)}, u32[]{:S(2)}) collective-permute-start(bf16[16,896]{1,0:T(8,128)(2,1)S(1)} %get-tuple-element.73), channel_id=1, source_target_pairs={{0,2},{1,3},{2,0},{3,1},{4,6},{5,7},{6,4},{7,5},{8,10},{9,11},{10,... | collective-permute-start | bytes 86024 | tf_op jit(solution)/shard_map/ppermute | solution.py:71
  77.2 2.2 %collective-permute-start.10 = (bf16[16,896]{1,0:T(8,128)(2,1)S(1)}, bf16[16,896]{1,0:T(8,128)(2,1)S(1)}, u32[]{:S(2)}, u32[]{:S(2)}) collective-permute-start(bf16[16,896]{1,0:T(8,128)(2,1)S(1)} %get-tuple-element.74), channel_id=1, source_target_pairs={{0,4},{1,5},{2,6},{3,7},{4,0},{5,1},{6,2},{7,3},{8,12},{9,13},{10,... | collective-permute-start | bytes 86024 | tf_op jit(solution)/shard_map/ppermute | solution.py:71
  79.4 0.6 collective-permute-start.11
  80.0 2.4 %shard_map.179 = (bf16[2,3,16,512]{3,2,1,0:T(8,128)(2,1)}, f32[2,16,4,64,128]{4,3,2,1,0:T(8,128)}) custom-call(s32[1,16]{1,0:T(1,128)S(1)} %bitcast.18, bf16[2,3,16,512]{3,2,1,0:T(8,128)(2,1)S(1)} %bitcast.8, f32[2,16,4,64,128]{4,3,2,1,0:T(8,128)S(1)} %copy-done, f32[16,256]{1,0:T(8,128)S(1)} %get-tuple-element.76.scaled_ref, ...), custom_call_target="tpu_custom_call" | custom-call | flops 2000000000 | bytes 4194304 | tf_op jit(solution)/shard_map/pallas_call | solution.py:444
  82.6 1.9 %collective-permute-done.11.refs_3_ = bf16[16,896]{1,0:T(8,128)(2,1)S(1)} collective-permute-done((bf16[16,896]{1,0:T(8,128)(2,1)S(1)}, bf16[16,896]{1,0:T(8,128)(2,1)S(1)}, u32[]{:S(2)}, u32[]{:S(2)}) %collective-permute-start.11) | collective-permute-done | bytes 28704 | tf_op jit(solution)/shard_map/ppermute | solution.py:71
  84.5 0.9 shard_map.180
  85.3 0.9 collective-permute-start.14
  86.4 3.4 %collective-permute-start.12 = (bf16[16,256]{1,0:T(8,128)(2,1)S(1)}, bf16[16,256]{1,0:T(8,128)(2,1)S(1)}, u32[]{:S(2)}, u32[]{:S(2)}) collective-permute-start(bf16[16,256]{1,0:T(8,128)(2,1)S(1)} %get-tuple-element.95.refs_0_), channel_id=1, source_target_pairs={{0,2},{1,3},{2,0},{3,1},{4,6},{5,7},{6,4},{7,5},{8,10},{9,11},{10,... | collective-permute-start | bytes 24584 | tf_op jit(solution)/shard_map/ppermute | solution.py:71
  89.7 2.4 %shard_map.181 = (bf16[2,3,16,512]{3,2,1,0:T(8,128)(2,1)}, f32[2,16,4,64,128]{4,3,2,1,0:T(8,128)}) custom-call(s32[1,16]{1,0:T(1,128)S(1)} %bitcast.20, bf16[2,3,16,512]{3,2,1,0:T(8,128)(2,1)S(1)} %bitcast.10, f32[2,16,4,64,128]{4,3,2,1,0:T(8,128)S(1)} %copy-done, ...), custom_call_target="tpu_custom_call", output_to_operand_aliasing={{0}: (7, {}), {1}: (8, {})} | custom-call | flops 2000000000 | bytes 4194304 | tf_op jit(solution)/shard_map/pallas_call | solution.py:444
  92.4 17.0 %all_to_all.22.parts_ref = bf16[16,8,512]{2,1,0:T(8,128)(2,1)S(1)} all-to-all(bf16[16,8,512]{2,1,0:T(8,128)(2,1)S(1)} %bitcast.13), channel_id=1, replica_groups=mesh['grp'=2,'tp'=16,'dp'=8] {'tp'}, dimensions={0} | all-to-all | bytes 262144 | tf_op jit(solution)/shard_map/all_to_all | solution.py:462
  109.4 16.9 %all_to_all.23.own_ref = bf16[16,8,512]{2,1,0:T(8,128)(2,1)S(1)} all-to-all(bf16[16,8,512]{2,1,0:T(8,128)(2,1)S(1)} %shard_map.183), channel_id=1, replica_groups=mesh['grp'=2,'tp'=16,'dp'=8] {'tp'}, dimensions={0} | all-to-all | bytes 262144 | tf_op jit(solution)/shard_map/all_to_all | solution.py:462
  126.3 1.2 collective-permute-done.15.other_ref
  127.6 0.7 order.1
  (52 shorter events, 2.0 us)
Async XLA Ops:
  0.6 0.9 copy-start.4
  0.6 1.0 copy-start.6
  0.7 1.1 copy-start.5
  0.7 1.2 copy-start.2
  0.7 1.4 %copy-start.3 = (bf16[2,512,256]{2,1,0:T(8,128)(2,1)S(1)}, bf16[2,512,256]{2,1,0:T(8,128)(2,1)}, u32[]{:S(2)}) copy-start(bf16[2,512,256]{2,1,0:T(8,128)(2,1)} %wz_ref.3) | copy-start | bytes 1572868
  0.7 1.4 %copy-start.10 = (f32[2,512]{1,0:T(2,128)S(1)}, f32[2,512]{1,0:T(2,128)}, u32[]{:S(2)}) copy-start(f32[2,512]{1,0:T(2,128)} %gain_ref.3) | copy-start | bytes 12292
  0.7 1.4 %copy-start.8 = (bf16[2,512,64]{1,2,0:T(8,128)(2,1)S(1)}, bf16[2,512,64]{1,2,0:T(8,128)(2,1)}, u32[]{:S(2)}) copy-start(bf16[2,512,64]{1,2,0:T(8,128)(2,1)} %param.23) | copy-start | bytes 393220
  0.7 2.0 %copy-start.1 = (bf16[2,256,512]{2,1,0:T(8,128)(2,1)S(1)}, bf16[2,256,512]{2,1,0:T(8,128)(2,1)}, u32[]{:S(2)}) copy-start(bf16[2,256,512]{2,1,0:T(8,128)(2,1)} %refs_4_.3) | copy-start | bytes 1572868
  2.5 1.4 %collective-permute-start = (bf16[64,896]{1,0:T(8,128)(2,1)S(1)}, bf16[64,896]{1,0:T(8,128)(2,1)S(1)}, u32[]{:S(2)}, u32[]{:S(2)}) collective-permute-start(bf16[64,896]{1,0:T(8,128)(2,1)S(1)} %project_away.1), channel_id=1, source_target_pairs={{0,1},{1,0},{2,3},{3,2},{4,5},{5,4},{6,7},{7,6},{8,9},{9,8},{10,11... | collective-permute-start | bytes 344072 | tf_op jit(solution)/shard_map/ppermute | solution.py:71
  2.7 18.1 %collective-permute-start.8 = (bf16[2,256,512]{2,1,0:T(8,128)(2,1)S(1)}, bf16[2,256,512]{2,1,0:T(8,128)(2,1)S(1)}, u32[]{:S(2)}, u32[]{:S(2)}) collective-permute-start(bf16[2,256,512]{2,1,0:T(8,128)(2,1)S(1)} %copy-done.1), channel_id=1, source_target_pairs={{0,1},{1,0},{2,3},{3,2},{4,5},{5,4},{6,7},{7,6},{8,9},{9,8},{10,11... | collective-permute-start | bytes 1572872 | tf_op jit(solution)/shard_map/ppermute | solution.py:71
  3.7 17.1 %collective-permute-start.7 = (bf16[656,896]{1,0:T(8,128)(2,1)S(1)}, bf16[656,896]{1,0:T(8,128)(2,1)S(1)}, u32[]{:S(2)}, u32[]{:S(2)}) collective-permute-start(bf16[656,896]{1,0:T(8,128)(2,1)S(1)} %get-tuple-element.58.own_ref), channel_id=1, source_target_pairs={{0,1},{1,0},{2,3},{3,2},{4,5},{5,4},{6,7},{7,6},{8,9},{9,8},{10,11... | collective-permute-start | bytes 3526664 | tf_op jit(solution)/shard_map/ppermute | solution.py:71
  4.0 5.0 %copy-start = (f32[2,16,4,64,128]{4,3,2,1,0:T(8,128)S(1)}, f32[2,16,4,64,128]{4,3,2,1,0:T(8,128)}, u32[]{:S(2)}) copy-start(f32[2,16,4,64,128]{4,3,2,1,0:T(8,128)} %state_ref.5) | copy-start | bytes 12582916
  4.1 5.6 %collective-permute-start.1 = (bf16[16,896]{1,0:T(8,128)(2,1)S(1)}, bf16[16,896]{1,0:T(8,128)(2,1)S(1)}, u32[]{:S(2)}, u32[]{:S(2)}) collective-permute-start(bf16[16,896]{1,0:T(8,128)(2,1)S(1)} %get-tuple-element.54), channel_id=1, source_target_pairs={{0,2},{1,3},{2,0},{3,1},{4,6},{5,7},{6,4},{7,5},{8,10},{9,11},{10,... | collective-permute-start | bytes 86024 | tf_op jit(solution)/shard_map/ppermute | solution.py:71
  5.9 5.4 %collective-permute-start.2 = (bf16[16,896]{1,0:T(8,128)(2,1)S(1)}, bf16[16,896]{1,0:T(8,128)(2,1)S(1)}, u32[]{:S(2)}, u32[]{:S(2)}) collective-permute-start(bf16[16,896]{1,0:T(8,128)(2,1)S(1)} %get-tuple-element.55), channel_id=1, source_target_pairs={{0,4},{1,5},{2,6},{3,7},{4,0},{5,1},{6,2},{7,3},{8,12},{9,13},{10,... | collective-permute-start | bytes 86024 | tf_op jit(solution)/shard_map/ppermute | solution.py:71
  8.9 5.1 %collective-permute-start.3 = (bf16[16,896]{1,0:T(8,128)(2,1)S(1)}, bf16[16,896]{1,0:T(8,128)(2,1)S(1)}, u32[]{:S(2)}, u32[]{:S(2)}) collective-permute-start(bf16[16,896]{1,0:T(8,128)(2,1)S(1)} %get-tuple-element.56), channel_id=1, source_target_pairs={{0,6},{1,7},{2,4},{3,5},{4,2},{5,3},{6,0},{7,1},{8,14},{9,15},{10,... | collective-permute-start | bytes 86024 | tf_op jit(solution)/shard_map/ppermute | solution.py:71
  9.0 5.0 %copy-start.7 = (bf16[2,16,3,512]{3,1,2,0:T(8,128)(2,1)S(1)}, bf16[2,16,3,512]{3,1,2,0:T(8,128)(2,1)}, u32[]{:S(2)}) copy-start(bf16[2,16,3,512]{3,1,2,0:T(8,128)(2,1)} %param.30) | copy-start | bytes 294916
  9.0 5.0 %copy-start.9 = (bf16[2,4,512]{2,1,0:T(4,128)(2,1)S(1)}, bf16[2,4,512]{2,1,0:T(4,128)(2,1)}, u32[]{:S(2)}) copy-start(bf16[2,4,512]{2,1,0:T(4,128)(2,1)} %refs_5_.3) | copy-start | bytes 24580
  9.0 5.0 %copy-start.11 = (f32[2,256]{1,0:T(2,128)S(1)}, f32[2,256]{1,0:T(2,128)}, u32[]{:S(2)}) copy-start(f32[2,256]{1,0:T(2,128)} %refs_9_.3) | copy-start | bytes 6148
  9.0 5.0 %copy-start.12 = (s32[16]{0:T(128)S(1)}, s32[16]{0:T(128)}, u32[]{:S(2)}) copy-start(s32[16]{0:T(128)} %param.17) | copy-start | bytes 196
  9.0 5.0 %copy-start.13 = (f32[2,4]{1,0:T(2,128)S(1)}, f32[2,4]{1,0:T(2,128)}, u32[]{:S(2)}) copy-start(f32[2,4]{1,0:T(2,128)} %refs_6_.3) | copy-start | bytes 100
  9.0 5.0 %copy-start.14 = (f32[2,4]{1,0:T(2,128)S(1)}, f32[2,4]{1,0:T(2,128)}, u32[]{:S(2)}) copy-start(f32[2,4]{1,0:T(2,128)} %refs_7_.3) | copy-start | bytes 100
  9.0 5.0 %copy-start.15 = (f32[2,4]{1,0:T(2,128)S(1)}, f32[2,4]{1,0:T(2,128)}, u32[]{:S(2)}) copy-start(f32[2,4]{1,0:T(2,128)} %refs_8_.3) | copy-start | bytes 100
  14.9 5.0 %collective-permute-start.6 = (bf16[16,256]{1,0:T(8,128)(2,1)S(1)}, bf16[16,256]{1,0:T(8,128)(2,1)S(1)}, u32[]{:S(2)}, u32[]{:S(2)}) collective-permute-start(bf16[16,256]{1,0:T(8,128)(2,1)S(1)} %get-tuple-element.59.refs_0_), channel_id=1, source_target_pairs={{0,6},{1,7},{2,4},{3,5},{4,2},{5,3},{6,0},{7,1},{8,14},{9,15},{10,... | collective-permute-start | bytes 24584 | tf_op jit(solution)/shard_map/ppermute | solution.py:71
  15.1 5.2 %collective-permute-start.5 = (bf16[16,256]{1,0:T(8,128)(2,1)S(1)}, bf16[16,256]{1,0:T(8,128)(2,1)S(1)}, u32[]{:S(2)}, u32[]{:S(2)}) collective-permute-start(bf16[16,256]{1,0:T(8,128)(2,1)S(1)} %get-tuple-element.59.refs_0_), channel_id=1, source_target_pairs={{0,4},{1,5},{2,6},{3,7},{4,0},{5,1},{6,2},{7,3},{8,12},{9,13},{10,... | collective-permute-start | bytes 24584 | tf_op jit(solution)/shard_map/ppermute | solution.py:71
  16.0 4.9 %collective-permute-start.4 = (bf16[16,256]{1,0:T(8,128)(2,1)S(1)}, bf16[16,256]{1,0:T(8,128)(2,1)S(1)}, u32[]{:S(2)}, u32[]{:S(2)}) collective-permute-start(bf16[16,256]{1,0:T(8,128)(2,1)S(1)} %get-tuple-element.59.refs_0_), channel_id=1, source_target_pairs={{0,2},{1,3},{2,0},{3,1},{4,6},{5,7},{6,4},{7,5},{8,10},{9,11},{10,... | collective-permute-start | bytes 24584 | tf_op jit(solution)/shard_map/ppermute | solution.py:71
  75.2 7.2 %collective-permute-start.9 = (bf16[16,896]{1,0:T(8,128)(2,1)S(1)}, bf16[16,896]{1,0:T(8,128)(2,1)S(1)}, u32[]{:S(2)}, u32[]{:S(2)}) collective-permute-start(bf16[16,896]{1,0:T(8,128)(2,1)S(1)} %get-tuple-element.73), channel_id=1, source_target_pairs={{0,2},{1,3},{2,0},{3,1},{4,6},{5,7},{6,4},{7,5},{8,10},{9,11},{10,... | collective-permute-start | bytes 86024 | tf_op jit(solution)/shard_map/ppermute | solution.py:71
  77.2 5.4 %collective-permute-start.10 = (bf16[16,896]{1,0:T(8,128)(2,1)S(1)}, bf16[16,896]{1,0:T(8,128)(2,1)S(1)}, u32[]{:S(2)}, u32[]{:S(2)}) collective-permute-start(bf16[16,896]{1,0:T(8,128)(2,1)S(1)} %get-tuple-element.74), channel_id=1, source_target_pairs={{0,4},{1,5},{2,6},{3,7},{4,0},{5,1},{6,2},{7,3},{8,12},{9,13},{10,... | collective-permute-start | bytes 86024 | tf_op jit(solution)/shard_map/ppermute | solution.py:71
  79.4 5.1 %collective-permute-start.11 = (bf16[16,896]{1,0:T(8,128)(2,1)S(1)}, bf16[16,896]{1,0:T(8,128)(2,1)S(1)}, u32[]{:S(2)}, u32[]{:S(2)}) collective-permute-start(bf16[16,896]{1,0:T(8,128)(2,1)S(1)} %get-tuple-element.75), channel_id=1, source_target_pairs={{0,6},{1,7},{2,4},{3,5},{4,2},{5,3},{6,0},{7,1},{8,14},{9,15},{10,... | collective-permute-start | bytes 86024 | tf_op jit(solution)/shard_map/ppermute | solution.py:71
  85.3 6.8 %collective-permute-start.14 = (bf16[16,256]{1,0:T(8,128)(2,1)S(1)}, bf16[16,256]{1,0:T(8,128)(2,1)S(1)}, u32[]{:S(2)}, u32[]{:S(2)}) collective-permute-start(bf16[16,256]{1,0:T(8,128)(2,1)S(1)} %get-tuple-element.95.refs_0_), channel_id=1, source_target_pairs={{0,6},{1,7},{2,4},{3,5},{4,2},{5,3},{6,0},{7,1},{8,14},{9,15},{10,... | collective-permute-start | bytes 24584 | tf_op jit(solution)/shard_map/ppermute | solution.py:71
  86.3 5.9 %collective-permute-start.13 = (bf16[16,256]{1,0:T(8,128)(2,1)S(1)}, bf16[16,256]{1,0:T(8,128)(2,1)S(1)}, u32[]{:S(2)}, u32[]{:S(2)}) collective-permute-start(bf16[16,256]{1,0:T(8,128)(2,1)S(1)} %get-tuple-element.95.refs_0_), channel_id=1, source_target_pairs={{0,4},{1,5},{2,6},{3,7},{4,0},{5,1},{6,2},{7,3},{8,12},{9,13},{10,... | collective-permute-start | bytes 24584 | tf_op jit(solution)/shard_map/ppermute | solution.py:71
  86.4 5.8 %collective-permute-start.12 = (bf16[16,256]{1,0:T(8,128)(2,1)S(1)}, bf16[16,256]{1,0:T(8,128)(2,1)S(1)}, u32[]{:S(2)}, u32[]{:S(2)}) collective-permute-start(bf16[16,256]{1,0:T(8,128)(2,1)S(1)} %get-tuple-element.95.refs_0_), channel_id=1, source_target_pairs={{0,2},{1,3},{2,0},{3,1},{4,6},{5,7},{6,4},{7,5},{8,10},{9,11},{10,... | collective-permute-start | bytes 24584 | tf_op jit(solution)/shard_map/ppermute | solution.py:71
  126.3 1.3 collective-permute-start.15

commit v2 on v1

--- a/solution.py
+++ b/solution.py
@@ -231,7 +231,7 @@
     past_ref = past_ref.at[layer]
     seqs = parts[0].shape[0]
     heads = bias_ref.shape[1]
-    width_x, width_n = state_ref.shape[2], state_ref.shape[3] // 2
+    width_x, width_n = state_ref.shape[2], state_ref.shape[3]
     head_dim = width_x // heads
     conv = width_x + 2 * width_n
     total = sum(part[...].astype(F32) for part in parts)
@@ -271,10 +271,7 @@
     keys_ref[...] = write_keys
     decay_ref[...] = decay
 
-    high, low = split(read_keys)
-    left = jnp.concatenate(
-        [jnp.concatenate([high, high], axis=1), jnp.concatenate([low, jnp.zeros_like(low)], axis=1)], axis=0
-    )
+    left = jnp.concatenate(split(read_keys), axis=0)
     seen = jnp.zeros((seqs, width_x), F32)
     for s in range(seqs):
         both = dot(left, state_ref[layer, s], ((1,), (1,)))
@@ -289,7 +286,7 @@
 
 def mix(layer, parts, lengths, taps, bias, alog, skip, gain, past, state):
     seqs = parts[0].shape[-2]
-    heads, width_x, width_n = bias.shape[1], state.shape[2], state.shape[3] // 2
+    heads, width_x, width_n = bias.shape[1], state.shape[2], state.shape[3]
     shapes = (
         jax.ShapeDtypeStruct((seqs, width_x), BF16),
         jax.ShapeDtypeStruct((seqs, width_x), F32),
@@ -387,16 +384,14 @@
     layers, seqs, heads, head_dim, width_n = state_ref.shape
     for layer in range(layers):
         for s in range(seqs):
-            high, low = split(state_ref[layer, s].reshape(heads * head_dim, width_n))
-            out_ref[layer, s, :, :width_n] = high
-            out_ref[layer, s, :, width_n:] = low
+            out_ref[layer, s] = state_ref[layer, s].reshape(heads * head_dim, width_n).astype(BF16)
 
 
 def prepare(after, state):
     layers, seqs, heads, head_dim, width_n = state.shape
     return pl.pallas_call(
         prepare_kernel,
-        out_shape=jax.ShapeDtypeStruct((layers, seqs, heads * head_dim, 2 * width_n), BF16),
+        out_shape=jax.ShapeDtypeStruct((layers, seqs, heads * head_dim, width_n), BF16),
         in_specs=[VMEM_SPEC] * 2,
         out_specs=VMEM_SPEC,
         compiler_params=params(12),

time: 130 us -> 129 us (level)
  no operation moved by 1% of the time
where the time goes in v2:
time: 129 us; the launch traced here: 128 us
  blocking collectives  87.5 us (68%)
  starting transfers between devices  18.9 us (15%)
  waiting for transfers between devices  9.8 us (8%)
  Pallas kernels  9.02 us (7%)
  local copies, waits for them, and re-layouts  1.45 us (1%)
    all_to_all x4, blocking collectives, exchange(): return lax.all_to_all(blocks, axis, 0, 0, tiled=True)  87.5 us
    ppermute x16, starting transfers between devices, swapped(): return lax.ppermute(value, 'dp', pairs)  18.9 us
    ppermute x16, waiting for transfers between devices, swapped(): return lax.ppermute(value, 'dp', pairs)  9.8 us
    pallas_call x2, Pallas kernels, states(): pl.pallas_call(functools.partial(states_kernel, layer, pieces), out_shape...  4.78 us
  transfers between devices with their start and end apart: 16, of which 8 were waited for; matrix products, arithmetic and copies ran while one was open for 0% of the time, Pallas kernels for 5%

profile of v2, /device:TPU:40, one launch (start us, length us, event | category | flops | bytes accessed | tf_op | source)
XLA Modules:
  0.0 127.7 jit_solution(18001184680897906118)
XLA Ops:
  0.7 0.8 copy-done.4
  2.1 0.4 project_away.1
  2.7 0.5 collective-permute-start.8
  3.2 0.5 project_home.1
  3.7 0.3 collective-permute-start.7
  4.2 1.7 %collective-permute-start.1 = (bf16[16,896]{1,0:T(8,128)(2,1)S(1)}, bf16[16,896]{1,0:T(8,128)(2,1)S(1)}, u32[]{:S(2)}, u32[]{:S(2)}) collective-permute-start(bf16[16,896]{1,0:T(8,128)(2,1)S(1)} %get-tuple-element.54), channel_id=1, source_target_pairs={{0,2},{1,3},{2,0},{3,1},{4,6},{5,7},{6,4},{7,5},{8,10},{9,11},{10,... | collective-permute-start | bytes 86024 | tf_op jit(solution)/shard_map/ppermute | solution.py:71
  6.0 3.0 %collective-permute-start.2 = (bf16[16,896]{1,0:T(8,128)(2,1)S(1)}, bf16[16,896]{1,0:T(8,128)(2,1)S(1)}, u32[]{:S(2)}, u32[]{:S(2)}) collective-permute-start(bf16[16,896]{1,0:T(8,128)(2,1)S(1)} %get-tuple-element.55), channel_id=1, source_target_pairs={{0,4},{1,5},{2,6},{3,7},{4,0},{5,1},{6,2},{7,3},{8,12},{9,13},{10,... | collective-permute-start | bytes 86024 | tf_op jit(solution)/shard_map/ppermute | solution.py:71
  9.1 0.2 prepare.1.refs_11_
  9.3 2.1 %collective-permute-done.2.refs_2_ = bf16[16,896]{1,0:T(8,128)(2,1)S(1)} collective-permute-done((bf16[16,896]{1,0:T(8,128)(2,1)S(1)}, bf16[16,896]{1,0:T(8,128)(2,1)S(1)}, u32[]{:S(2)}, u32[]{:S(2)}) %collective-permute-start.2) | collective-permute-done | bytes 28704 | tf_op jit(solution)/shard_map/ppermute | solution.py:71
  11.4 2.7 %collective-permute-done.3.refs_3_ = bf16[16,896]{1,0:T(8,128)(2,1)S(1)} collective-permute-done((bf16[16,896]{1,0:T(8,128)(2,1)S(1)}, bf16[16,896]{1,0:T(8,128)(2,1)S(1)}, u32[]{:S(2)}, u32[]{:S(2)}) %collective-permute-start.3) | collective-permute-done | bytes 28704 | tf_op jit(solution)/shard_map/ppermute | solution.py:71
  14.1 0.7 shard_map.175
  15.0 0.9 collective-permute-start.5
  15.8 3.1 %collective-permute-start.4 = (bf16[16,256]{1,0:T(8,128)(2,1)S(1)}, bf16[16,256]{1,0:T(8,128)(2,1)S(1)}, u32[]{:S(2)}, u32[]{:S(2)}) collective-permute-start(bf16[16,256]{1,0:T(8,128)(2,1)S(1)} %get-tuple-element.59.refs_0_), channel_id=1, source_target_pairs={{0,2},{1,3},{2,0},{3,1},{4,6},{5,7},{6,4},{7,5},{8,10},{9,11},{10,... | collective-permute-start | bytes 24584 | tf_op jit(solution)/shard_map/ppermute | solution.py:71
  19.0 0.8 collective-permute-done.6.refs_3_
  19.7 0.4 collective-permute-done.5.refs_2_
  20.2 0.5 collective-permute-done.4.refs_1_
  20.9 36.7 %all_to_all.20.parts_ref = bf16[16,8,512]{2,1,0:T(8,128)(2,1)S(1)} all-to-all(bf16[16,8,512]{2,1,0:T(8,128)(2,1)S(1)} %bitcast.14), channel_id=1, replica_groups=mesh['grp'=2,'tp'=16,'dp'=8] {'tp'}, dimensions={0} | all-to-all | bytes 262144 | tf_op jit(solution)/shard_map/all_to_all | solution.py:457
  57.7 17.0 %all_to_all.21 = bf16[16,8,512]{2,1,0:T(8,128)(2,1)S(1)} all-to-all(bf16[16,8,512]{2,1,0:T(8,128)(2,1)S(1)} %shard_map.177), channel_id=1, replica_groups=mesh['grp'=2,'tp'=16,'dp'=8] {'tp'}, dimensions={0} | all-to-all | bytes 262144 | tf_op jit(solution)/shard_map/all_to_all | solution.py:457
  74.6 0.4 shard_map.178
  75.1 2.0 %collective-permute-start.9 = (bf16[16,896]{1,0:T(8,128)(2,1)S(1)}, bf16[16,896]{1,0:T(8,128)(2,1)S(1)}, u32[]{:S(2)}, u32[]{:S(2)}) collective-permute-start(bf16[16,896]{1,0:T(8,128)(2,1)S(1)} %get-tuple-element.73), channel_id=1, source_target_pairs={{0,2},{1,3},{2,0},{3,1},{4,6},{5,7},{6,4},{7,5},{8,10},{9,11},{10,... | collective-permute-start | bytes 86024 | tf_op jit(solution)/shard_map/ppermute | solution.py:71
  77.1 2.2 %collective-permute-start.10 = (bf16[16,896]{1,0:T(8,128)(2,1)S(1)}, bf16[16,896]{1,0:T(8,128)(2,1)S(1)}, u32[]{:S(2)}, u32[]{:S(2)}) collective-permute-start(bf16[16,896]{1,0:T(8,128)(2,1)S(1)} %get-tuple-element.74), channel_id=1, source_target_pairs={{0,4},{1,5},{2,6},{3,7},{4,0},{5,1},{6,2},{7,3},{8,12},{9,13},{10,... | collective-permute-start | bytes 86024 | tf_op jit(solution)/shard_map/ppermute | solution.py:71
  79.2 0.6 collective-permute-start.11
  79.9 2.4 %shard_map.179 = (bf16[2,3,16,512]{3,2,1,0:T(8,128)(2,1)}, f32[2,16,4,64,128]{4,3,2,1,0:T(8,128)}) custom-call(s32[1,16]{1,0:T(1,128)S(1)} %bitcast.18, bf16[2,3,16,512]{3,2,1,0:T(8,128)(2,1)S(1)} %bitcast.8, f32[2,16,4,64,128]{4,3,2,1,0:T(8,128)S(1)} %copy-done, f32[16,256]{1,0:T(8,128)S(1)} %get-tuple-element.76.scaled_ref, ...), custom_call_target="tpu_custom_call" | custom-call | flops 2000000000 | bytes 4194304 | tf_op jit(solution)/shard_map/pallas_call | solution.py:439
  82.4 1.9 %collective-permute-done.11.refs_3_ = bf16[16,896]{1,0:T(8,128)(2,1)S(1)} collective-permute-done((bf16[16,896]{1,0:T(8,128)(2,1)S(1)}, bf16[16,896]{1,0:T(8,128)(2,1)S(1)}, u32[]{:S(2)}, u32[]{:S(2)}) %collective-permute-start.11) | collective-permute-done | bytes 28704 | tf_op jit(solution)/shard_map/ppermute | solution.py:71
  84.3 0.7 shard_map.180
  85.0 0.7 collective-permute-start.14
  85.8 3.4 %collective-permute-start.12 = (bf16[16,256]{1,0:T(8,128)(2,1)S(1)}, bf16[16,256]{1,0:T(8,128)(2,1)S(1)}, u32[]{:S(2)}, u32[]{:S(2)}) collective-permute-start(bf16[16,256]{1,0:T(8,128)(2,1)S(1)} %get-tuple-element.95.refs_0_), channel_id=1, source_target_pairs={{0,2},{1,3},{2,0},{3,1},{4,6},{5,7},{6,4},{7,5},{8,10},{9,11},{10,... | collective-permute-start | bytes 24584 | tf_op jit(solution)/shard_map/ppermute | solution.py:71
  89.2 2.4 %shard_map.181 = (bf16[2,3,16,512]{3,2,1,0:T(8,128)(2,1)}, f32[2,16,4,64,128]{4,3,2,1,0:T(8,128)}) custom-call(s32[1,16]{1,0:T(1,128)S(1)} %bitcast.20, bf16[2,3,16,512]{3,2,1,0:T(8,128)(2,1)S(1)} %bitcast.10, f32[2,16,4,64,128]{4,3,2,1,0:T(8,128)S(1)} %copy-done, ...), custom_call_target="tpu_custom_call", output_to_operand_aliasing={{0}: (7, {}), {1}: (8, {})} | custom-call | flops 2000000000 | bytes 4194304 | tf_op jit(solution)/shard_map/pallas_call | solution.py:439
  91.8 17.0 %all_to_all.22.parts_ref = bf16[16,8,512]{2,1,0:T(8,128)(2,1)S(1)} all-to-all(bf16[16,8,512]{2,1,0:T(8,128)(2,1)S(1)} %bitcast.13), channel_id=1, replica_groups=mesh['grp'=2,'tp'=16,'dp'=8] {'tp'}, dimensions={0} | all-to-all | bytes 262144 | tf_op jit(solution)/shard_map/all_to_all | solution.py:457
  108.8 16.9 %all_to_all.23.own_ref = bf16[16,8,512]{2,1,0:T(8,128)(2,1)S(1)} all-to-all(bf16[16,8,512]{2,1,0:T(8,128)(2,1)S(1)} %shard_map.183), channel_id=1, replica_groups=mesh['grp'=2,'tp'=16,'dp'=8] {'tp'}, dimensions={0} | all-to-all | bytes 262144 | tf_op jit(solution)/shard_map/all_to_all | solution.py:457
  125.8 1.2 collective-permute-done.15.other_ref
  127.0 0.7 order.1
  (52 shorter events, 1.9 us)
Async XLA Ops:
  0.6 0.9 copy-start.4
  0.6 1.0 copy-start.6
  0.7 1.1 copy-start.5
  0.7 1.2 copy-start.2
  0.7 1.4 %copy-start.3 = (bf16[2,512,256]{2,1,0:T(8,128)(2,1)S(1)}, bf16[2,512,256]{2,1,0:T(8,128)(2,1)}, u32[]{:S(2)}) copy-start(bf16[2,512,256]{2,1,0:T(8,128)(2,1)} %wz_ref.3) | copy-start | bytes 1572868
  0.7 1.4 %copy-start.10 = (f32[2,512]{1,0:T(2,128)S(1)}, f32[2,512]{1,0:T(2,128)}, u32[]{:S(2)}) copy-start(f32[2,512]{1,0:T(2,128)} %gain_ref.3) | copy-start | bytes 12292
  0.7 1.4 %copy-start.8 = (bf16[2,512,64]{1,2,0:T(8,128)(2,1)S(1)}, bf16[2,512,64]{1,2,0:T(8,128)(2,1)}, u32[]{:S(2)}) copy-start(bf16[2,512,64]{1,2,0:T(8,128)(2,1)} %param.23) | copy-start | bytes 393220
  0.7 2.0 %copy-start.1 = (bf16[2,256,512]{2,1,0:T(8,128)(2,1)S(1)}, bf16[2,256,512]{2,1,0:T(8,128)(2,1)}, u32[]{:S(2)}) copy-start(bf16[2,256,512]{2,1,0:T(8,128)(2,1)} %refs_4_.3) | copy-start | bytes 1572868
  2.5 1.4 %collective-permute-start = (bf16[64,896]{1,0:T(8,128)(2,1)S(1)}, bf16[64,896]{1,0:T(8,128)(2,1)S(1)}, u32[]{:S(2)}, u32[]{:S(2)}) collective-permute-start(bf16[64,896]{1,0:T(8,128)(2,1)S(1)} %project_away.1), channel_id=1, source_target_pairs={{0,1},{1,0},{2,3},{3,2},{4,5},{5,4},{6,7},{7,6},{8,9},{9,8},{10,11... | collective-permute-start | bytes 344072 | tf_op jit(solution)/shard_map/ppermute | solution.py:71
  2.7 18.0 %collective-permute-start.8 = (bf16[2,256,512]{2,1,0:T(8,128)(2,1)S(1)}, bf16[2,256,512]{2,1,0:T(8,128)(2,1)S(1)}, u32[]{:S(2)}, u32[]{:S(2)}) collective-permute-start(bf16[2,256,512]{2,1,0:T(8,128)(2,1)S(1)} %copy-done.1), channel_id=1, source_target_pairs={{0,1},{1,0},{2,3},{3,2},{4,5},{5,4},{6,7},{7,6},{8,9},{9,8},{10,11... | collective-permute-start | bytes 1572872 | tf_op jit(solution)/shard_map/ppermute | solution.py:71
  3.7 17.0 %collective-permute-start.7 = (bf16[656,896]{1,0:T(8,128)(2,1)S(1)}, bf16[656,896]{1,0:T(8,128)(2,1)S(1)}, u32[]{:S(2)}, u32[]{:S(2)}) collective-permute-start(bf16[656,896]{1,0:T(8,128)(2,1)S(1)} %get-tuple-element.58.own_ref), channel_id=1, source_target_pairs={{0,1},{1,0},{2,3},{3,2},{4,5},{5,4},{6,7},{7,6},{8,9},{9,8},{10,11... | collective-permute-start | bytes 3526664 | tf_op jit(solution)/shard_map/ppermute | solution.py:71
  4.0 5.1 %copy-start = (f32[2,16,4,64,128]{4,3,2,1,0:T(8,128)S(1)}, f32[2,16,4,64,128]{4,3,2,1,0:T(8,128)}, u32[]{:S(2)}) copy-start(f32[2,16,4,64,128]{4,3,2,1,0:T(8,128)} %state_ref.5) | copy-start | bytes 12582916
  4.1 9.9 %copy-start.7 = (bf16[2,16,3,512]{3,1,2,0:T(8,128)(2,1)S(1)}, bf16[2,16,3,512]{3,1,2,0:T(8,128)(2,1)}, u32[]{:S(2)}) copy-start(bf16[2,16,3,512]{3,1,2,0:T(8,128)(2,1)} %param.30) | copy-start | bytes 294916
  4.2 9.9 %copy-start.9 = (bf16[2,4,512]{2,1,0:T(4,128)(2,1)S(1)}, bf16[2,4,512]{2,1,0:T(4,128)(2,1)}, u32[]{:S(2)}) copy-start(bf16[2,4,512]{2,1,0:T(4,128)(2,1)} %refs_5_.3) | copy-start | bytes 24580
  4.2 9.9 %copy-start.11 = (f32[2,256]{1,0:T(2,128)S(1)}, f32[2,256]{1,0:T(2,128)}, u32[]{:S(2)}) copy-start(f32[2,256]{1,0:T(2,128)} %refs_9_.3) | copy-start | bytes 6148
  4.2 9.9 %copy-start.12 = (s32[16]{0:T(128)S(1)}, s32[16]{0:T(128)}, u32[]{:S(2)}) copy-start(s32[16]{0:T(128)} %param.17) | copy-start | bytes 196
  4.2 9.9 %copy-start.13 = (f32[2,4]{1,0:T(2,128)S(1)}, f32[2,4]{1,0:T(2,128)}, u32[]{:S(2)}) copy-start(f32[2,4]{1,0:T(2,128)} %refs_6_.3) | copy-start | bytes 100
  4.2 9.9 %copy-start.14 = (f32[2,4]{1,0:T(2,128)S(1)}, f32[2,4]{1,0:T(2,128)}, u32[]{:S(2)}) copy-start(f32[2,4]{1,0:T(2,128)} %refs_7_.3) | copy-start | bytes 100
  4.2 9.9 %copy-start.15 = (f32[2,4]{1,0:T(2,128)S(1)}, f32[2,4]{1,0:T(2,128)}, u32[]{:S(2)}) copy-start(f32[2,4]{1,0:T(2,128)} %refs_8_.3) | copy-start | bytes 100
  4.2 5.0 %collective-permute-start.1 = (bf16[16,896]{1,0:T(8,128)(2,1)S(1)}, bf16[16,896]{1,0:T(8,128)(2,1)S(1)}, u32[]{:S(2)}, u32[]{:S(2)}) collective-permute-start(bf16[16,896]{1,0:T(8,128)(2,1)S(1)} %get-tuple-element.54), channel_id=1, source_target_pairs={{0,2},{1,3},{2,0},{3,1},{4,6},{5,7},{6,4},{7,5},{8,10},{9,11},{10,... | collective-permute-start | bytes 86024 | tf_op jit(solution)/shard_map/ppermute | solution.py:71
  6.0 5.4 %collective-permute-start.2 = (bf16[16,896]{1,0:T(8,128)(2,1)S(1)}, bf16[16,896]{1,0:T(8,128)(2,1)S(1)}, u32[]{:S(2)}, u32[]{:S(2)}) collective-permute-start(bf16[16,896]{1,0:T(8,128)(2,1)S(1)} %get-tuple-element.55), channel_id=1, source_target_pairs={{0,4},{1,5},{2,6},{3,7},{4,0},{5,1},{6,2},{7,3},{8,12},{9,13},{10,... | collective-permute-start | bytes 86024 | tf_op jit(solution)/shard_map/ppermute | solution.py:71
  9.0 5.1 %collective-permute-start.3 = (bf16[16,896]{1,0:T(8,128)(2,1)S(1)}, bf16[16,896]{1,0:T(8,128)(2,1)S(1)}, u32[]{:S(2)}, u32[]{:S(2)}) collective-permute-start(bf16[16,896]{1,0:T(8,128)(2,1)S(1)} %get-tuple-element.56), channel_id=1, source_target_pairs={{0,6},{1,7},{2,4},{3,5},{4,2},{5,3},{6,0},{7,1},{8,14},{9,15},{10,... | collective-permute-start | bytes 86024 | tf_op jit(solution)/shard_map/ppermute | solution.py:71
  14.8 4.9 %collective-permute-start.6 = (bf16[16,256]{1,0:T(8,128)(2,1)S(1)}, bf16[16,256]{1,0:T(8,128)(2,1)S(1)}, u32[]{:S(2)}, u32[]{:S(2)}) collective-permute-start(bf16[16,256]{1,0:T(8,128)(2,1)S(1)} %get-tuple-element.59.refs_0_), channel_id=1, source_target_pairs={{0,6},{1,7},{2,4},{3,5},{4,2},{5,3},{6,0},{7,1},{8,14},{9,15},{10,... | collective-permute-start | bytes 24584 | tf_op jit(solution)/shard_map/ppermute | solution.py:71
  15.0 5.2 %collective-permute-start.5 = (bf16[16,256]{1,0:T(8,128)(2,1)S(1)}, bf16[16,256]{1,0:T(8,128)(2,1)S(1)}, u32[]{:S(2)}, u32[]{:S(2)}) collective-permute-start(bf16[16,256]{1,0:T(8,128)(2,1)S(1)} %get-tuple-element.59.refs_0_), channel_id=1, source_target_pairs={{0,4},{1,5},{2,6},{3,7},{4,0},{5,1},{6,2},{7,3},{8,12},{9,13},{10,... | collective-permute-start | bytes 24584 | tf_op jit(solution)/shard_map/ppermute | solution.py:71
  15.8 4.9 %collective-permute-start.4 = (bf16[16,256]{1,0:T(8,128)(2,1)S(1)}, bf16[16,256]{1,0:T(8,128)(2,1)S(1)}, u32[]{:S(2)}, u32[]{:S(2)}) collective-permute-start(bf16[16,256]{1,0:T(8,128)(2,1)S(1)} %get-tuple-element.59.refs_0_), channel_id=1, source_target_pairs={{0,2},{1,3},{2,0},{3,1},{4,6},{5,7},{6,4},{7,5},{8,10},{9,11},{10,... | collective-permute-start | bytes 24584 | tf_op jit(solution)/shard_map/ppermute | solution.py:71
  75.1 7.2 %collective-permute-start.9 = (bf16[16,896]{1,0:T(8,128)(2,1)S(1)}, bf16[16,896]{1,0:T(8,128)(2,1)S(1)}, u32[]{:S(2)}, u32[]{:S(2)}) collective-permute-start(bf16[16,896]{1,0:T(8,128)(2,1)S(1)} %get-tuple-element.73), channel_id=1, source_target_pairs={{0,2},{1,3},{2,0},{3,1},{4,6},{5,7},{6,4},{7,5},{8,10},{9,11},{10,... | collective-permute-start | bytes 86024 | tf_op jit(solution)/shard_map/ppermute | solution.py:71
  77.1 5.4 %collective-permute-start.10 = (bf16[16,896]{1,0:T(8,128)(2,1)S(1)}, bf16[16,896]{1,0:T(8,128)(2,1)S(1)}, u32[]{:S(2)}, u32[]{:S(2)}) collective-permute-start(bf16[16,896]{1,0:T(8,128)(2,1)S(1)} %get-tuple-element.74), channel_id=1, source_target_pairs={{0,4},{1,5},{2,6},{3,7},{4,0},{5,1},{6,2},{7,3},{8,12},{9,13},{10,... | collective-permute-start | bytes 86024 | tf_op jit(solution)/shard_map/ppermute | solution.py:71
  79.2 5.1 %collective-permute-start.11 = (bf16[16,896]{1,0:T(8,128)(2,1)S(1)}, bf16[16,896]{1,0:T(8,128)(2,1)S(1)}, u32[]{:S(2)}, u32[]{:S(2)}) collective-permute-start(bf16[16,896]{1,0:T(8,128)(2,1)S(1)} %get-tuple-element.75), channel_id=1, source_target_pairs={{0,6},{1,7},{2,4},{3,5},{4,2},{5,3},{6,0},{7,1},{8,14},{9,15},{10,... | collective-permute-start | bytes 86024 | tf_op jit(solution)/shard_map/ppermute | solution.py:71
  85.0 6.6 %collective-permute-start.14 = (bf16[16,256]{1,0:T(8,128)(2,1)S(1)}, bf16[16,256]{1,0:T(8,128)(2,1)S(1)}, u32[]{:S(2)}, u32[]{:S(2)}) collective-permute-start(bf16[16,256]{1,0:T(8,128)(2,1)S(1)} %get-tuple-element.95.refs_0_), channel_id=1, source_target_pairs={{0,6},{1,7},{2,4},{3,5},{4,2},{5,3},{6,0},{7,1},{8,14},{9,15},{10,... | collective-permute-start | bytes 24584 | tf_op jit(solution)/shard_map/ppermute | solution.py:71
  85.7 5.9 %collective-permute-start.13 = (bf16[16,256]{1,0:T(8,128)(2,1)S(1)}, bf16[16,256]{1,0:T(8,128)(2,1)S(1)}, u32[]{:S(2)}, u32[]{:S(2)}) collective-permute-start(bf16[16,256]{1,0:T(8,128)(2,1)S(1)} %get-tuple-element.95.refs_0_), channel_id=1, source_target_pairs={{0,4},{1,5},{2,6},{3,7},{4,0},{5,1},{6,2},{7,3},{8,12},{9,13},{10,... | collective-permute-start | bytes 24584 | tf_op jit(solution)/shard_map/ppermute | solution.py:71
  85.8 5.8 %collective-permute-start.12 = (bf16[16,256]{1,0:T(8,128)(2,1)S(1)}, bf16[16,256]{1,0:T(8,128)(2,1)S(1)}, u32[]{:S(2)}, u32[]{:S(2)}) collective-permute-start(bf16[16,256]{1,0:T(8,128)(2,1)S(1)} %get-tuple-element.95.refs_0_), channel_id=1, source_target_pairs={{0,2},{1,3},{2,0},{3,1},{4,6},{5,7},{6,4},{7,5},{8,10},{9,11},{10,... | collective-permute-start | bytes 24584 | tf_op jit(solution)/shard_map/ppermute | solution.py:71
  125.7 1.3 collective-permute-start.15
